TPU v7x, 128 devices: a whole 4x4x4 slice. The times are simulated.
128 devices in a mesh: rep: 16 (over z, x), fs: 4 (over y), tp: 2 (over core).
Axes of the slice: x: 4, y: 4, z: 4, core: 2. Of those that a mesh axis runs over, the one named last changes fastest.
Arguments:
- inputs: bfloat16 [64, 768, 2048], P(('rep', 'fs'), 'tp'), may hold values from -6 to 6
- pre_gate: bfloat16 [64, 768, 2816], P(('rep', 'fs'), None, 'tp'), may hold values from -6 to 6
- pre_up: bfloat16 [64, 768, 2816], P(('rep', 'fs'), None, 'tp'), may hold values from -6 to 6
- cotangent: bfloat16 [64, 768, 2816], P(('rep', 'fs'), None, 'tp'), may hold values from -16 to 16
- w_gate: bfloat16 [2048, 2816], P('fs', 'tp'), may hold values from -0.125 to 0.125
- w_up: bfloat16 [2048, 2816], P('fs', 'tp'), may hold values from -0.125 to 0.125
- taps_gate: bfloat16 [3, 2816], replicated, may hold values from -3 to 3
- taps_up: bfloat16 [3, 2816], replicated, may hold values from -3 to 3
Outputs:
- grad_inputs: bfloat16 [64, 768, 2048], P(('rep', 'fs'), 'tp')
- grad_w_gate: float32 [2048, 2816], P('fs', 'tp')
- grad_w_up: float32 [2048, 2816], P('fs', 'tp')
- grad_taps_gate: float32 [3, 2816], replicated
- grad_taps_up: float32 [3, 2816], replicated
All inputs are finite; a program needn't handle non-finite values.
Results may differ from a plain program's by a relative error of at most 0.0059.
Values may be sent and summed in bfloat16 or wider, within the bound.
A program may use at most 192 MiB of HBM per device.

v0:
```python
import functools

import jax
import jax.numpy as jnp
from jax import lax
from jax.experimental import pallas as pl
from jax.experimental.pallas import tpu as pltpu
from jax.sharding import PartitionSpec as P

F32 = jnp.float32
BF16 = jnp.bfloat16
MESH = pl.DeviceIdType.MESH

Y1, Y3, X1, X3, Z1, Z3 = range(6)
CYCLE = (X1, Z1, X3, Z3, Y1, Y3)
REP_CYCLE = (X1, Z1, X3, Z3)
GROUPS = ((0, 512), (512, 512), (1024, 384))
SUB = 32
PORTIONS = tuple((group, mat) for group in range(3) for mat in range(2))
ORDERS = tuple(tuple(CYCLE[(p + s) % 6] for s in range(6)) for p in range(6))
AG_START = (0, 1, 2, 3, 0, 2)
AG_ORDERS = tuple(tuple(REP_CYCLE[(a + t) % 4] for t in range(4)) for a in AG_START)
LEN = 768
HALF = 384
D = 2048
FC = 1408
W_PATHS = ((Y1, Y3), (Y3, Y1))
MASK = {Y1: 1, Y3: 3}


def recv_offset(stage):
    return 64 - 2 ** (6 - stage)


def kernel(
    x_hbm, gate_hbm, up_hbm, cot_hbm, wg_hbm, wu_hbm, kg_ref, ku_ref,
    gin_hbm, gwg_hbm, gwu_hbm, taps_hbm,
    xs, xt, act_g, act_u, act_c, ws_g, ws_u,
    g0, g1, g2, g3, g4, g5, r0, r1, r2, r3, r4, r5, a0, a1, a2, a3, a4, a5,
    stage_g, stage_u, tap, tap_in, tap_out, part, part_in,
    load_sem, rs_send, rs_recv, ag_send, ag_recv, wy_send, wy_recv, wf_send, wf_recv,
    t_send, t_recv, x_send, x_recv, o_send, o_recv, out_sem,
):
    gs, rs, ags = (g0, g1, g2, g3, g4, g5), (r0, r1, r2, r3, r4, r5), (a0, a1, a2, a3, a4, a5)
    ws = (ws_g, ws_u)
    acts = (act_g, act_u)
    stages = (stage_g, stage_u)
    rep, y, tp = lax.axis_index("rep"), lax.axis_index("fs"), lax.axis_index("tp")
    z, x = rep // 4, rep % 4

    def gray(c):
        return (c + c // 2) % 2, c // 2

    bits = gray(y) + gray(x) + gray(z)

    def flip1(c):
        return c + 1 - 2 * (c % 2)

    peers = (
        {"fs": flip1(y)}, {"fs": 3 - y},
        {"rep": z * 4 + flip1(x)}, {"rep": z * 4 + 3 - x},
        {"rep": flip1(z) * 4 + x}, {"rep": (3 - z) * 4 + x},
    )
    other_core = {"tp": 1 - tp}
    pending = []

    def remote(src, dst, send, recv, peer):
        return pltpu.make_async_remote_copy(
            src_ref=src, dst_ref=dst, send_sem=send, recv_sem=recv, device_id=peer, device_id_type=MESH
        )

    def send(copy):
        copy.start()
        pending.append(copy)

    loads = {}

    def load(name, src, dst):
        copy = pltpu.make_async_copy(src, dst, load_sem.at[len(loads)])
        copy.start()
        loads[name] = copy

    load("x", x_hbm, xs.at[tp])
    for mat, src in enumerate((wg_hbm, wu_hbm)):
        load("w" + str(mat), src, ws[mat].at[0])
    for group, (first, size) in enumerate(GROUPS):
        for name, src, dst in (("g", gate_hbm, act_g), ("u", up_hbm, act_u), ("c", cot_hbm, act_c)):
            load(name + str(group), src.at[:, pl.ds(first, size)], dst.at[:, pl.ds(first, size)])

    barrier = pltpu.get_barrier_semaphore()
    for peer in peers + (other_core,):
        pl.semaphore_signal(barrier, inc=1, device_id=peer, device_id_type=MESH)
    pl.semaphore_wait(barrier, 7)

    parity = (x % 2, z % 2)

    def wy_index(mat, mask, axis):
        return (mat * 3 + mask - 1) * 2 + axis

    def wy_copy(mat, src_mask, dim, axis):
        dst_mask = src_mask ^ MASK[dim]
        at = wy_index(mat, dst_mask, axis)
        return remote(
            ws[mat].at[src_mask, pl.ds(2 * axis, 2), parity[axis]],
            ws[mat].at[dst_mask, pl.ds(2 * axis, 2), parity[axis]],
            wy_send.at[at], wy_recv.at[at], peers[dim],
        )

    def wf_copy(mat, mask, link):
        at = (mat * 3 + mask - 1) * 4 + link
        half = ws[mat].at[mask, link, parity[link // 2]]
        return remote(half, half, wf_send.at[at], wf_recv.at[at], peers[2 + link])

    def w_own(mat, step, axis):
        send(wy_copy(mat, 0, W_PATHS[mat][step], axis))

    def w_wait_y(mat, step, relayed, axis):
        dim = W_PATHS[mat][step]
        src = MASK[W_PATHS[mat][0]] if relayed else 0
        wy_copy(mat, src, dim, axis).wait_recv()

    def w_relay(mat, axis):
        send(wy_copy(mat, MASK[W_PATHS[mat][0]], W_PATHS[mat][1], axis))

    def w_forward(mat, mask, axis):
        for link in (2 * axis, 2 * axis + 1):
            send(wf_copy(mat, mask, link))

    def w_done(mask):
        for mat in range(2):
            for link in range(4):
                wf_copy(mat, mask, link).wait_recv()

    row = lax.broadcasted_iota(jnp.int32, (LEN, 128), 0)

    def past(value, steps):
        return jnp.where(row >= steps, pltpu.roll(value, steps, 0), 0.0)

    def ahead(value, steps):
        return jnp.where(row < LEN - steps, pltpu.roll(value, LEN - steps, 0), 0.0)

    def elementwise(group):
        first, size = GROUPS[group]
        for name in ("g", "u", "c"):
            loads[name + str(group)].wait()

        def block(j, _):
            cols = pl.ds(pl.multiple_of(first + j * 128, 128), 128)
            tap_cols = pl.ds(pl.multiple_of(tp * FC + first + j * 128, 128), 128)
            kg_all = kg_ref[:, tap_cols].astype(F32)
            ku_all = ku_ref[:, tap_cols].astype(F32)
            kg = [kg_all[i : i + 1, :] for i in range(3)]
            ku = [ku_all[i : i + 1, :] for i in range(3)]
            gate = act_g[:, cols].astype(F32)
            gates = (past(gate, 2), past(gate, 1), gate)
            mixed_gate = kg[0] * gates[0] + kg[1] * gates[1] + kg[2] * gates[2]
            up = act_u[:, cols].astype(F32)
            ups = (past(up, 2), past(up, 1), up)
            mixed_up = ku[0] * ups[0] + ku[1] * ups[1] + ku[2] * ups[2]
            scale = (2.0 / 3.141592653589793) ** 0.5
            square = mixed_gate * mixed_gate
            bent = jnp.tanh(mixed_gate * (scale + (scale * 0.044715) * square))
            lift = 0.5 + 0.5 * bent
            slope = lift + mixed_gate * (1.0 - bent * bent) * (0.5 * scale + (1.5 * 0.044715 * scale) * square)
            cot = act_c[:, cols].astype(F32)
            back_up = cot * (mixed_gate * lift)
            back_gate = cot * mixed_up * slope
            dg = kg[2] * back_gate + kg[1] * ahead(back_gate, 1) + kg[0] * ahead(back_gate, 2)
            du = ku[2] * back_up + ku[1] * ahead(back_up, 1) + ku[0] * ahead(back_up, 2)
            act_g[:, cols] = dg.astype(BF16)
            act_u[:, cols] = du.astype(BF16)
            for i in range(3):
                tap[0, pl.ds(i, 1), cols] = jnp.sum(back_gate * gates[i], axis=0, keepdims=True)
                tap[0, pl.ds(3 + i, 1), cols] = jnp.sum(back_up * ups[i], axis=0, keepdims=True)
            return 0

        lax.fori_loop(0, size // 128, block, 0)

    def product(p):
        group, mat = PORTIONS[p]
        first, size = GROUPS[group]
        weights_at = {ORDERS[p][s]: 2 ** (5 - s) for s in range(6)}

        def block(yb, _):
            value = jnp.dot(
                xt[pl.ds(pl.multiple_of(yb * 512, 512), 512), :],
                acts[mat][:, pl.ds(first, size)],
                preferred_element_type=F32,
            ).astype(BF16)
            low, high = gray(yb)
            base = low * weights_at[Y1] + high * weights_at[Y3]
            for sub in range(16):
                at = sum(((sub >> k) & 1) * weights_at[2 + k] for k in range(4))
                gs[p][base + at] = value[sub * SUB : (sub + 1) * SUB, :]
            return 0

        lax.fori_loop(0, 4, block, 0)

    def base_of(p, stage):
        return sum(bits[ORDERS[p][s]] * 2 ** (5 - s) for s in range(stage))

    def rs_copy(p, stage):
        dim, count = ORDERS[p][stage], 2 ** (5 - stage)
        start = base_of(p, stage) + (1 - bits[dim]) * count
        at = p * 6 + stage
        return remote(
            gs[p].at[pl.ds(start, count)], rs[p].at[pl.ds(recv_offset(stage), count)],
            rs_send.at[at], rs_recv.at[at], peers[dim],
        )

    def ag_at(p):
        return sum(bits[dim] * 2**t for t, dim in enumerate(AG_ORDERS[p]))

    def ag_copy(p, step):
        count = 2**step
        held = ags[p].at[pl.ds((ag_at(p) // count) * count, count)]
        at = p * 4 + step
        return remote(held, held, ag_send.at[at], ag_recv.at[at], peers[AG_ORDERS[p][step]])

    def first_send(p):
        send(rs_copy(p, 0))

    def rs_step(p, stage):
        rs_copy(p, stage).wait_recv()
        start, count, offset = base_of(p, stage + 1), 2 ** (5 - stage), recv_offset(stage)

        def total(i):
            return (gs[p][start + i].astype(F32) + rs[p][offset + i].astype(F32)).astype(BF16)

        if stage == 5:
            ags[p][ag_at(p)] = total(0)
            send(ag_copy(p, 0))
            return

        def add(i, _):
            gs[p][start + i] = total(i)
            return 0

        lax.fori_loop(0, count, add, 0)
        send(rs_copy(p, stage + 1))

    def ag_step(p, step):
        ag_copy(p, step).wait_recv()
        if step < 3:
            send(ag_copy(p, step + 1))
            return
        group, mat = PORTIONS[p]
        first, size = GROUPS[group]
        for sub in range(16):
            at = sum(((sub >> (dim - 2)) & 1) * 2**t for t, dim in enumerate(AG_ORDERS[p]))
            stages[mat][pl.ds(sub * SUB, SUB), pl.ds(first, size)] = ags[p][at]

    def tap_copy(step):
        peer = peers[step] if step < 6 else other_core
        return remote(tap.at[step], tap_in.at[step], t_send.at[step], t_recv.at[step], peer)

    def tap_step(step):
        if step >= 0:
            tap_copy(step).wait_recv()
            tap[step + 1] = tap[step] + tap_in[step]
        send(tap_copy(step + 1))

    def back(mask):
        def block(n, _):
            def dot(mat):
                weights = ws[mat][mask, pl.ds(2 * n, 2)].reshape(256, FC)
                return lax.dot_general(
                    acts[mat][...], weights, (((1,), (1,)), ((), ())), preferred_element_type=F32
                )

            value = (dot(0) + dot(1)).astype(BF16)
            cols = pl.ds(pl.multiple_of(n * 256, 256), 256)
            part[mask, 0, :, cols] = value[:HALF]
            part[mask, 1, :, cols] = value[HALF:]
            return 0

        lax.fori_loop(0, 2, block, 0)
        send(part_copy(mask))

    def part_copy(mask):
        return remote(
            part.at[mask, 1 - tp], part_in.at[mask], o_send.at[mask], o_recv.at[mask], other_core
        )

    outs = []

    def finish(mask):
        part_copy(mask).wait_recv()
        part_in[mask] = (part[mask, tp].astype(F32) + part_in[mask].astype(F32)).astype(BF16)
        block = {0: y, 1: flip1(y), 2: (y + 2) % 4, 3: 3 - y}[mask]
        copy = pltpu.make_async_copy(
            part_in.at[mask],
            gin_hbm.at[:, pl.ds(pl.multiple_of(block * 512, 512), 512)],
            out_sem.at[len(outs)],
        )
        copy.start()
        outs.append(copy)

    def store(src, dst):
        copy = pltpu.make_async_copy(src, dst, out_sem.at[len(outs)])
        copy.start()
        outs.append(copy)

    loads["w0"].wait()
    loads["w1"].wait()
    for mat in range(2):
        for axis in range(2):
            w_own(mat, 0, axis)
    loads["x"].wait()
    x_copy = remote(xs.at[tp], xs.at[tp], x_send.at[0], x_recv.at[0], other_core)
    send(x_copy)
    tap[0] = jnp.zeros((8, FC), F32)

    elementwise(0)
    x_copy.wait_recv()

    def turn(c, _):
        cols = pl.ds(pl.multiple_of(c * 128, 128), 128)
        for h in range(2):
            xt[cols, pl.ds(h * HALF, HALF)] = xs[h, :, cols].T
        return 0

    lax.fori_loop(0, D // 128, turn, 0)
    product(0)
    first_send(0)
    product(1)
    first_send(1)
    elementwise(1)
    product(2)
    first_send(2)
    product(3)
    first_send(3)
    for axis in range(2):
        for mat in range(2):
            w_own(mat, 1, axis)
    elementwise(2)
    product(4)
    first_send(4)
    product(5)
    first_send(5)
    tap_step(-1)
    for axis in range(2):
        for mat in range(2):
            w_wait_y(mat, 0, False, axis)
            w_relay(mat, axis)
    back(0)
    rs_step(0, 0)
    rs_step(1, 0)
    for mat in range(2):
        for axis in range(2):
            w_forward(mat, MASK[W_PATHS[mat][0]], axis)
    rs_step(2, 0)
    rs_step(3, 0)
    tap_step(0)
    finish(0)
    rs_step(0, 1)
    rs_step(1, 1)
    rs_step(4, 0)
    rs_step(5, 0)
    for mat in range(2):
        for axis in range(2):
            w_wait_y(mat, 1, False, axis)
            w_forward(mat, MASK[W_PATHS[mat][1]], axis)
    tap_step(1)
    for p in range(4):
        rs_step(p, 2 if p < 2 else 1)
    rs_step(4, 1)
    rs_step(5, 1)
    tap_step(2)
    for p in range(4):
        rs_step(p, 3 if p < 2 else 2)
    rs_step(4, 2)
    rs_step(5, 2)
    tap_step(3)
    for p in range(4):
        rs_step(p, 4 if p < 2 else 3)
    rs_step(4, 3)
    rs_step(5, 3)
    tap_step(4)
    for p in range(4):
        rs_step(p, 5 if p < 2 else 4)
    rs_step(4, 4)
    rs_step(5, 4)
    for mat in range(2):
        for axis in range(2):
            w_wait_y(mat, 1, True, axis)
            w_forward(mat, 2, axis)
    rs_step(2, 5)
    rs_step(3, 5)
    rs_step(4, 5)
    rs_step(5, 5)
    tap_step(5)
    for step in range(3):
        for p in range(6):
            ag_step(p, step)
    w_done(1)
    back(1)
    w_done(3)
    back(3)
    finish(1)
    finish(3)
    for p in range(6):
        ag_step(p, 3)
    store(stage_g, gwg_hbm)
    store(stage_u, gwu_hbm)
    w_done(2)
    back(2)
    tap_copy(6).wait_recv()
    tap_out[tp] = tap[6]
    tap_out[1 - tp] = tap_in[6]
    store(tap_out, taps_hbm)
    finish(2)
    for copy in pending:
        copy.wait_send()
    for copy in outs:
        copy.wait()


def fused(x, gate, up, cot, wg, wu, kg, ku):
    sizes = [GROUPS[group][1] for group, _ in PORTIONS]
    any_space = pl.BlockSpec(memory_space=pl.ANY)
    in_vmem = pl.BlockSpec(memory_space=pltpu.VMEM)
    dma = pltpu.SemaphoreType.DMA
    return pl.pallas_call(
        kernel,
        in_specs=[any_space] * 6 + [in_vmem] * 2,
        out_specs=[any_space] * 4,
        out_shape=[
            jax.ShapeDtypeStruct((HALF, D), BF16),
            jax.ShapeDtypeStruct((512, FC), BF16),
            jax.ShapeDtypeStruct((512, FC), BF16),
            jax.ShapeDtypeStruct((2, 8, FC), F32),
        ],
        scratch_shapes=[
            pltpu.VMEM((2, HALF, D), BF16),
            pltpu.VMEM((D, LEN), BF16),
            pltpu.VMEM((LEN, FC), BF16),
            pltpu.VMEM((LEN, FC), BF16),
            pltpu.VMEM((LEN, FC), BF16),
            pltpu.VMEM((4, 4, 2, 64, FC), BF16),
            pltpu.VMEM((4, 4, 2, 64, FC), BF16),
        ]
        + [pltpu.VMEM((64, SUB, size), BF16) for size in sizes]
        + [pltpu.VMEM((63, SUB, size), BF16) for size in sizes]
        + [pltpu.VMEM((16, SUB, size), BF16) for size in sizes]
        + [
            pltpu.VMEM((512, FC), BF16),
            pltpu.VMEM((512, FC), BF16),
            pltpu.VMEM((7, 8, FC), F32),
            pltpu.VMEM((7, 8, FC), F32),
            pltpu.VMEM((2, 8, FC), F32),
            pltpu.VMEM((4, 2, HALF, 512), BF16),
            pltpu.VMEM((4, HALF, 512), BF16),
            dma((12,)), dma((36,)), dma((36,)), dma((24,)), dma((24,)),
            dma((12,)), dma((12,)), dma((24,)), dma((24,)),
            dma((7,)), dma((7,)), dma((1,)), dma((1,)), dma((4,)), dma((4,)), dma((7,)),
        ],
        compiler_params=pltpu.CompilerParams(
            collective_id=0, has_side_effects=True, vmem_limit_bytes=67043328
        ),
        cost_estimate=pl.CostEstimate(flops=18 * 10**9, bytes_accessed=20 * 2**20, transcendentals=10**6),
    )(x, gate, up, cot, wg, wu, kg, ku)


def per_device(inputs, pre_gate, pre_up, cotangent, w_gate, w_up, taps_gate, taps_up):
    count = LEN * lax.axis_size("rep") * lax.axis_size("fs")
    factor = float(count) ** (-0.5)
    grad_inputs, grad_gate, grad_up, taps = fused(
        inputs[0], pre_gate[0], pre_up[0], cotangent[0],
        w_gate.reshape(4, 2, 64, FC), w_up.reshape(4, 2, 64, FC), taps_gate, taps_up,
    )
    taps = factor * jnp.concatenate([taps[0], taps[1]], axis=1)
    return (
        grad_inputs[None],
        grad_gate.astype(F32) * factor,
        grad_up.astype(F32) * factor,
        taps[:3],
        taps[3:6],
    )


def solution(mesh):
    placed = (
        P(("rep", "fs"), "tp", None),
        P(("rep", "fs"), None, "tp"),
        P(("rep", "fs"), None, "tp"),
        P(("rep", "fs"), None, "tp"),
        P("fs", "tp"),
        P("fs", "tp"),
        P(),
        P(),
    )
    return jax.shard_map(
        per_device,
        mesh=mesh,
        in_specs=placed,
        out_specs=(P(("rep", "fs"), "tp", None), P("fs", "tp"), P("fs", "tp"), P(), P()),
        check_vma=False,
    )
```

profile of v0, /device:TPU:1, one launch (start us, length us, event | category | flops | bytes accessed | tf_op | source)
XLA Modules:
  0.0 149.6 jit_solution(15470293733460908204)
XLA Ops:
  0.6 141.4 %shard_map.119 = (bf16[384,2048]{1,0:T(8,128)(2,1)}, bf16[512,1408]{1,0:T(8,128)(2,1)}, bf16[512,1408]{1,0:T(8,128)(2,1)}, f32[2,8,1408]{2,1,0:T(8,128)}) custom-call(bf16[384,2048]{1,0:T(8,128)(2,1)} %bitcast.15, bf16[768,1408]{1,0:T(8,128)(2,1)} %bitcast.12, bf16[768,1408]{1,0:T(8,128)(2,1)} %bitcast.13, bf16[768,1408]{1,0:T(8,128)(2,1)} %bitcast.14, ...), custom_call_target="tpu_custom_call" | custom-call | flops 17999998976 | bytes 20971520 | tf_op jit(solution)/shard_map/pallas_call | solution.py:424
  142.0 0.8 slice_bitcast_fusion.1
  142.8 0.7 fusion
  143.5 0.0 copy-start
  143.5 5.0 %convert_multiply_fusion = (f32[512,1408]{1,0:T(8,128)}, f32[512,1408]{1,0:T(8,128)}) fusion(bf16[512,1408]{1,0:T(8,128)(2,1)} %get-tuple-element.11, bf16[512,1408]{1,0:T(8,128)(2,1)} %get-tuple-element.10), kind=kLoop, calls=%fused_computation | loop fusion | flops 2883584 | bytes 8650752 | tf_op jit(solution)/shard_map/mul | solution.py:476
  148.4 0.0 copy-done
  148.4 1.1 copy.14
  (1 shorter events, 0.0 us)
Async XLA Ops:
  143.5 5.0 %copy-start = (bf16[384,2048]{1,0:T(8,128)(2,1)S(1)}, bf16[384,2048]{1,0:T(8,128)(2,1)}, u32[]{:S(2)}) copy-start(bf16[384,2048]{1,0:T(8,128)(2,1)} %get-tuple-element.9) | copy-start | bytes 4718596
where the time goes:
time: 150 us
  Pallas kernels  141 us (94%)
  other arithmetic  4.96 us (3%)
  local copies, waits for them, and re-layouts  2.62 us (2%)
    pallas_call x1, Pallas kernels, fused(): pl.pallas_call(kernel, in_specs=[any_space] * 6 + [in_vmem] * 2, out_spec...  141 us
    mul x1, other arithmetic, per_device(): grad_up.astype(F32) * factor  4.95 us

commit v1 on v0

--- a/solution.py
+++ b/solution.py
@@ -15,11 +15,22 @@
 CYCLE = (X1, Z1, X3, Z3, Y1, Y3)
 REP_CYCLE = (X1, Z1, X3, Z3)
 GROUPS = ((0, 512), (512, 512), (1024, 384))
+SPLIT = 2
 SUB = 32
-PORTIONS = tuple((group, mat) for group in range(3) for mat in range(2))
-ORDERS = tuple(tuple(CYCLE[(p + s) % 6] for s in range(6)) for p in range(6))
-AG_START = (0, 1, 2, 3, 0, 2)
-AG_ORDERS = tuple(tuple(REP_CYCLE[(a + t) % 4] for t in range(4)) for a in AG_START)
+ROWS = SUB // SPLIT
+PORTIONS = tuple((group, mat, h) for group in range(3) for mat in range(2) for h in range(SPLIT))
+COUNT = len(PORTIONS)
+GROUP_ORDER = (0, 2, 1)
+ORDERS = (
+    (X1, Z1, X3, Z3, Y1, Y3), (Z1, X1, Y1, Z3, Y3, X3), (Z3, Y1, Y3, X1, Z1, X3), (X3, Z3, X1, Y3, Y1, Z1),
+    (X3, Z3, Y1, Y3, X1, Z1), (X1, Z1, X3, Z3, Y1, Y3), (Z3, Y1, Z1, X1, X3, Y3), (Z1, X3, Z3, Y1, X1, Y3),
+    (Y1, Y3, X1, Z1, X3, Z3), (Y3, X1, Z1, Y1, Z3, X3), (Y1, Y3, Z1, X1, X3, Z3), (Y3, X3, Z1, Z3, X1, Y1),
+)
+AG_ORDERS = (
+    (X1, X3, Z1, Z3), (X1, Z3, Z1, X3), (Z3, X3, Z1, X1), (Z1, X1, Z3, X3), (X3, Z3, Z1, X1),
+    (Z3, Z1, X1, X3), (Z3, X3, X1, Z1), (X1, Z1, Z3, X3), (X3, Z1, Z3, X1), (Z3, X3, X1, Z1),
+    (Z1, X3, Z3, X1), (Z1, Z3, X1, X3),
+)
 LEN = 768
 HALF = 384
 D = 2048
@@ -32,16 +43,51 @@
     return 64 - 2 ** (6 - stage)
 
 
+START, ELEM, TURN, PROD, RS, AG, WY, WF, TAP, BACK, FIN = range(11)
+NAMES = ("start", "elem", "turn", "prod", "rs", "ag", "wy", "wf", "tap", "back", "fin")
+SCHEDULE = (
+    (ELEM, 0, 0, 2), (START,), (WY, 0, 0, Y1, 0), (WY, 1, 0, Y3, 0), (ELEM, 0, 2, 4), (WY, 0, 0, Y1, 1),
+    (WY, 1, 0, Y3, 1), (TURN,), (PROD, 0, 0), (WY, 0, 0, Y1, 2), (WY, 1, 0, Y3, 2), (PROD, 0, 1),
+    (WY, 0, 0, Y1, 3), (WY, 1, 0, Y3, 3), (ELEM, 2, 0, 2), (ELEM, 2, 2, 3), (PROD, 2, 0), (PROD, 2, 1),
+    (ELEM, 1, 0, 2), (WF, 0, 1, 0), (WF, 0, 1, 2), (ELEM, 1, 2, 4), (WF, 0, 1, 1), (WF, 0, 1, 3),
+    (PROD, 1, 0), (TAP, -1), (WF, 1, 3, 2), (PROD, 1, 1), (RS, 1, 0), (RS, 3, 0), (RS, 2, 0), (RS, 0, 0),
+    (RS, 8, 0), (RS, 9, 0), (BACK, 0), (FIN, 0), (RS, 10, 0), (WF, 1, 3, 1), (RS, 11, 0), (RS, 5, 0),
+    (WY, 1, 3, Y1, 0), (TAP, 0), (RS, 4, 0), (RS, 6, 0), (RS, 8, 1), (WY, 0, 1, Y3, 0), (RS, 7, 0),
+    (RS, 2, 1), (RS, 1, 1), (RS, 10, 1), (RS, 3, 1), (RS, 0, 1), (WF, 1, 3, 3), (RS, 9, 1), (WY, 0, 1, Y3, 1),
+    (RS, 11, 1), (TAP, 1), (WF, 1, 3, 0), (RS, 8, 2), (WY, 1, 3, Y1, 1), (RS, 4, 1), (WY, 0, 1, Y3, 2),
+    (RS, 6, 1), (RS, 2, 2), (RS, 3, 2), (RS, 5, 1), (RS, 7, 1), (WF, 0, 2, 0), (RS, 1, 2), (RS, 10, 2),
+    (WF, 0, 2, 1), (TAP, 2), (RS, 0, 2), (RS, 9, 2), (WY, 0, 1, Y3, 3), (WY, 1, 3, Y1, 2), (RS, 2, 3),
+    (RS, 7, 2), (RS, 11, 2), (RS, 5, 2), (WF, 1, 2, 0), (WF, 0, 2, 2), (RS, 1, 3), (WF, 1, 2, 1), (RS, 8, 3),
+    (RS, 3, 3), (RS, 0, 3), (RS, 4, 2), (RS, 11, 3), (RS, 9, 3), (RS, 6, 2), (WY, 0, 0, Y3, 0), (RS, 10, 3),
+    (RS, 2, 4), (RS, 5, 3), (WF, 0, 2, 3), (RS, 9, 4), (RS, 1, 4), (WY, 1, 3, Y1, 3), (WF, 1, 2, 2),
+    (WY, 0, 0, Y3, 1), (TAP, 3), (RS, 4, 3), (RS, 7, 3), (RS, 11, 4), (RS, 8, 4), (RS, 3, 4), (RS, 10, 4),
+    (RS, 0, 4), (RS, 6, 3), (RS, 2, 5), (RS, 9, 5), (RS, 5, 4), (RS, 1, 5), (RS, 4, 4), (WY, 1, 0, Y1, 0),
+    (RS, 7, 4), (WF, 0, 3, 0), (RS, 8, 5), (RS, 10, 5), (AG, 2, 0), (WY, 0, 0, Y3, 2), (AG, 9, 0), (RS, 6, 4),
+    (AG, 1, 0), (AG, 8, 0), (RS, 3, 5), (WF, 1, 2, 3), (WY, 1, 0, Y1, 1), (RS, 4, 5), (RS, 11, 5),
+    (AG, 10, 0), (AG, 2, 1), (WF, 0, 3, 1), (AG, 9, 1), (RS, 0, 5), (AG, 1, 1), (RS, 5, 5), (RS, 7, 5),
+    (WY, 0, 0, Y3, 3), (AG, 8, 1), (TAP, 4), (AG, 4, 0), (AG, 3, 0), (AG, 11, 0), (AG, 10, 1),
+    (WY, 1, 0, Y1, 2), (WF, 1, 1, 0), (AG, 2, 2), (AG, 9, 2), (AG, 0, 0), (AG, 7, 0), (AG, 1, 2), (BACK, 2),
+    (WY, 1, 0, Y1, 3), (WF, 1, 1, 1), (WF, 0, 3, 2), (RS, 6, 5), (AG, 5, 0), (AG, 0, 1), (AG, 3, 1),
+    (AG, 8, 2), (AG, 9, 3), (AG, 4, 1), (AG, 7, 1), (AG, 11, 1), (WF, 0, 3, 3), (FIN, 2), (AG, 10, 2),
+    (AG, 1, 3), (AG, 6, 0), (TAP, 5), (AG, 3, 2), (AG, 2, 3), (AG, 7, 2), (WF, 1, 1, 2), (AG, 8, 3),
+    (AG, 6, 1), (AG, 5, 1), (WF, 1, 1, 3), (AG, 11, 2), (AG, 0, 2), (BACK, 3), (AG, 4, 2), (AG, 6, 2),
+    (AG, 3, 3), (AG, 10, 3), (AG, 5, 2), (AG, 7, 3), (BACK, 1), (FIN, 3), (AG, 0, 3), (AG, 11, 3), (AG, 4, 3),
+    (AG, 6, 3), (AG, 5, 3), (FIN, 1),
+)
+
+
 def kernel(
     x_hbm, gate_hbm, up_hbm, cot_hbm, wg_hbm, wu_hbm, kg_ref, ku_ref,
     gin_hbm, gwg_hbm, gwu_hbm, taps_hbm,
     xs, xt, act_g, act_u, act_c, ws_g, ws_u,
-    g0, g1, g2, g3, g4, g5, r0, r1, r2, r3, r4, r5, a0, a1, a2, a3, a4, a5,
-    stage_g, stage_u, tap, tap_in, tap_out, part, part_in,
-    load_sem, rs_send, rs_recv, ag_send, ag_recv, wy_send, wy_recv, wf_send, wf_recv,
-    t_send, t_recv, x_send, x_recv, o_send, o_recv, out_sem,
+    *scratch,
 ):
-    gs, rs, ags = (g0, g1, g2, g3, g4, g5), (r0, r1, r2, r3, r4, r5), (a0, a1, a2, a3, a4, a5)
+    gs, rs, ags = (scratch[i * COUNT : (i + 1) * COUNT] for i in range(3))
+    (
+        stage_g, stage_u, tap, tap_in, tap_out, part, part_in,
+        load_sem, rs_send, rs_recv, ag_send, ag_recv, wy_send, wy_recv, wf_send, wf_recv,
+        t_send, t_recv, x_send, x_recv, o_send, o_recv, out_sem,
+    ) = scratch[3 * COUNT :]
     ws = (ws_g, ws_u)
     acts = (act_g, act_u)
     stages = (stage_g, stage_u)
@@ -80,29 +126,30 @@
         copy.start()
         loads[name] = copy
 
+    def load_group(group):
+        first, size = GROUPS[group]
+        for name, src, dst in (("g", gate_hbm, act_g), ("u", up_hbm, act_u), ("c", cot_hbm, act_c)):
+            load(name + str(group), src.at[:, pl.ds(first, size)], dst.at[:, pl.ds(first, size)])
+
+    barrier = pltpu.get_barrier_semaphore()
+    for peer in peers + (other_core,):
+        pl.semaphore_signal(barrier, inc=1, device_id=peer, device_id_type=MESH)
+    load_group(GROUP_ORDER[0])
     load("x", x_hbm, xs.at[tp])
     for mat, src in enumerate((wg_hbm, wu_hbm)):
         load("w" + str(mat), src, ws[mat].at[0])
-    for group, (first, size) in enumerate(GROUPS):
-        for name, src, dst in (("g", gate_hbm, act_g), ("u", up_hbm, act_u), ("c", cot_hbm, act_c)):
-            load(name + str(group), src.at[:, pl.ds(first, size)], dst.at[:, pl.ds(first, size)])
-
-    barrier = pltpu.get_barrier_semaphore()
-    for peer in peers + (other_core,):
-        pl.semaphore_signal(barrier, inc=1, device_id=peer, device_id_type=MESH)
-    pl.semaphore_wait(barrier, 7)
+    load_group(GROUP_ORDER[1])
+    load_group(GROUP_ORDER[2])
+    tap[0] = jnp.zeros((8, FC), F32)
 
     parity = (x % 2, z % 2)
 
-    def wy_index(mat, mask, axis):
-        return (mat * 3 + mask - 1) * 2 + axis
-
-    def wy_copy(mat, src_mask, dim, axis):
+    def wy_copy(mat, src_mask, dim, link):
         dst_mask = src_mask ^ MASK[dim]
-        at = wy_index(mat, dst_mask, axis)
+        at = (mat * 3 + dst_mask - 1) * 4 + link
+        half = parity[link // 2]
         return remote(
-            ws[mat].at[src_mask, pl.ds(2 * axis, 2), parity[axis]],
-            ws[mat].at[dst_mask, pl.ds(2 * axis, 2), parity[axis]],
+            ws[mat].at[src_mask, link, half], ws[mat].at[dst_mask, link, half],
             wy_send.at[at], wy_recv.at[at], peers[dim],
         )
 
@@ -111,25 +158,23 @@
         half = ws[mat].at[mask, link, parity[link // 2]]
         return remote(half, half, wf_send.at[at], wf_recv.at[at], peers[2 + link])
 
-    def w_own(mat, step, axis):
-        send(wy_copy(mat, 0, W_PATHS[mat][step], axis))
-
-    def w_wait_y(mat, step, relayed, axis):
-        dim = W_PATHS[mat][step]
-        src = MASK[W_PATHS[mat][0]] if relayed else 0
-        wy_copy(mat, src, dim, axis).wait_recv()
-
-    def w_relay(mat, axis):
-        send(wy_copy(mat, MASK[W_PATHS[mat][0]], W_PATHS[mat][1], axis))
-
-    def w_forward(mat, mask, axis):
-        for link in (2 * axis, 2 * axis + 1):
-            send(wf_copy(mat, mask, link))
-
-    def w_done(mask):
-        for mat in range(2):
-            for link in range(4):
-                wf_copy(mat, mask, link).wait_recv()
+    waited = set()
+
+    def wy_wait(mat, mask, link):
+        first, second = W_PATHS[mat]
+        dim, src = {MASK[first]: (first, 0), MASK[second]: (second, 0), 2: (second, MASK[first])}[mask]
+        if (mat, mask, link) not in waited:
+            waited.add((mat, mask, link))
+            wy_copy(mat, src, dim, link).wait_recv()
+
+    def wy_step(mat, src_mask, dim, link):
+        if src_mask:
+            wy_wait(mat, src_mask, link)
+        send(wy_copy(mat, src_mask, dim, link))
+
+    def wf_step(mat, mask, link):
+        wy_wait(mat, mask, link)
+        send(wf_copy(mat, mask, link))
 
     row = lax.broadcasted_iota(jnp.int32, (LEN, 128), 0)
 
@@ -139,10 +184,11 @@
     def ahead(value, steps):
         return jnp.where(row < LEN - steps, pltpu.roll(value, LEN - steps, 0), 0.0)
 
-    def elementwise(group):
+    def elementwise(group, begin, end):
         first, size = GROUPS[group]
-        for name in ("g", "u", "c"):
-            loads[name + str(group)].wait()
+        if begin == 0:
+            for name in ("g", "u", "c"):
+                loads[name + str(group)].wait()
 
         def block(j, _):
             cols = pl.ds(pl.multiple_of(first + j * 128, 128), 128)
@@ -174,12 +220,12 @@
                 tap[0, pl.ds(3 + i, 1), cols] = jnp.sum(back_up * ups[i], axis=0, keepdims=True)
             return 0
 
-        lax.fori_loop(0, size // 128, block, 0)
-
-    def product(p):
-        group, mat = PORTIONS[p]
+        lax.fori_loop(begin, end, block, 0)
+
+    def product(group, mat):
         first, size = GROUPS[group]
-        weights_at = {ORDERS[p][s]: 2 ** (5 - s) for s in range(6)}
+        mine = [p for p in range(COUNT) if PORTIONS[p][:2] == (group, mat)]
+        places = [{ORDERS[p][s]: 2 ** (5 - s) for s in range(6)} for p in mine]
 
         def block(yb, _):
             value = jnp.dot(
@@ -188,13 +234,18 @@
                 preferred_element_type=F32,
             ).astype(BF16)
             low, high = gray(yb)
-            base = low * weights_at[Y1] + high * weights_at[Y3]
-            for sub in range(16):
-                at = sum(((sub >> k) & 1) * weights_at[2 + k] for k in range(4))
-                gs[p][base + at] = value[sub * SUB : (sub + 1) * SUB, :]
+            for h, p in enumerate(mine):
+                place = places[h]
+                base = low * place[Y1] + high * place[Y3]
+                for sub in range(16):
+                    at = sum(((sub >> k) & 1) * place[2 + k] for k in range(4))
+                    row_at = sub * SUB + h * ROWS
+                    gs[p][base + at] = value[row_at : row_at + ROWS, :]
             return 0
 
         lax.fori_loop(0, 4, block, 0)
+        for p in mine:
+            send(rs_copy(p, 0))
 
     def base_of(p, stage):
         return sum(bits[ORDERS[p][s]] * 2 ** (5 - s) for s in range(stage))
@@ -217,9 +268,6 @@
         at = p * 4 + step
         return remote(held, held, ag_send.at[at], ag_recv.at[at], peers[AG_ORDERS[p][step]])
 
-    def first_send(p):
-        send(rs_copy(p, 0))
-
     def rs_step(p, stage):
         rs_copy(p, stage).wait_recv()
         start, count, offset = base_of(p, stage + 1), 2 ** (5 - stage), recv_offset(stage)
@@ -244,11 +292,11 @@
         if step < 3:
             send(ag_copy(p, step + 1))
             return
-        group, mat = PORTIONS[p]
+        group, mat, h = PORTIONS[p]
         first, size = GROUPS[group]
         for sub in range(16):
             at = sum(((sub >> (dim - 2)) & 1) * 2**t for t, dim in enumerate(AG_ORDERS[p]))
-            stages[mat][pl.ds(sub * SUB, SUB), pl.ds(first, size)] = ags[p][at]
+            stages[mat][pl.ds(sub * SUB + h * ROWS, ROWS), pl.ds(first, size)] = ags[p][at]
 
     def tap_copy(step):
         peer = peers[step] if step < 6 else other_core
@@ -261,6 +309,12 @@
         send(tap_copy(step + 1))
 
     def back(mask):
+        for mat in range(2):
+            for link in range(4):
+                if mask:
+                    wy_wait(mat, mask, link)
+                    wf_copy(mat, mask, link).wait_recv()
+
         def block(n, _):
             def dot(mat):
                 weights = ws[mat][mask, pl.ds(2 * n, 2)].reshape(256, FC)
@@ -301,115 +355,38 @@
         copy.start()
         outs.append(copy)
 
-    loads["w0"].wait()
-    loads["w1"].wait()
-    for mat in range(2):
-        for axis in range(2):
-            w_own(mat, 0, axis)
-    loads["x"].wait()
+    def turn():
+        x_copy.wait_recv()
+
+        def block(c, _):
+            cols = pl.ds(pl.multiple_of(c * 128, 128), 128)
+            for h in range(2):
+                xt[cols, pl.ds(h * HALF, HALF)] = xs[h, :, cols].T
+            return 0
+
+        lax.fori_loop(0, D // 128, block, 0)
+
+    def start():
+        pl.semaphore_wait(barrier, 7)
+        loads["x"].wait()
+        send(x_copy)
+        loads["w0"].wait()
+        loads["w1"].wait()
+
     x_copy = remote(xs.at[tp], xs.at[tp], x_send.at[0], x_recv.at[0], other_core)
-    send(x_copy)
-    tap[0] = jnp.zeros((8, FC), F32)
-
-    elementwise(0)
-    x_copy.wait_recv()
-
-    def turn(c, _):
-        cols = pl.ds(pl.multiple_of(c * 128, 128), 128)
-        for h in range(2):
-            xt[cols, pl.ds(h * HALF, HALF)] = xs[h, :, cols].T
-        return 0
-
-    lax.fori_loop(0, D // 128, turn, 0)
-    product(0)
-    first_send(0)
-    product(1)
-    first_send(1)
-    elementwise(1)
-    product(2)
-    first_send(2)
-    product(3)
-    first_send(3)
-    for axis in range(2):
-        for mat in range(2):
-            w_own(mat, 1, axis)
-    elementwise(2)
-    product(4)
-    first_send(4)
-    product(5)
-    first_send(5)
-    tap_step(-1)
-    for axis in range(2):
-        for mat in range(2):
-            w_wait_y(mat, 0, False, axis)
-            w_relay(mat, axis)
-    back(0)
-    rs_step(0, 0)
-    rs_step(1, 0)
-    for mat in range(2):
-        for axis in range(2):
-            w_forward(mat, MASK[W_PATHS[mat][0]], axis)
-    rs_step(2, 0)
-    rs_step(3, 0)
-    tap_step(0)
-    finish(0)
-    rs_step(0, 1)
-    rs_step(1, 1)
-    rs_step(4, 0)
-    rs_step(5, 0)
-    for mat in range(2):
-        for axis in range(2):
-            w_wait_y(mat, 1, False, axis)
-            w_forward(mat, MASK[W_PATHS[mat][1]], axis)
-    tap_step(1)
-    for p in range(4):
-        rs_step(p, 2 if p < 2 else 1)
-    rs_step(4, 1)
-    rs_step(5, 1)
-    tap_step(2)
-    for p in range(4):
-        rs_step(p, 3 if p < 2 else 2)
-    rs_step(4, 2)
-    rs_step(5, 2)
-    tap_step(3)
-    for p in range(4):
-        rs_step(p, 4 if p < 2 else 3)
-    rs_step(4, 3)
-    rs_step(5, 3)
-    tap_step(4)
-    for p in range(4):
-        rs_step(p, 5 if p < 2 else 4)
-    rs_step(4, 4)
-    rs_step(5, 4)
-    for mat in range(2):
-        for axis in range(2):
-            w_wait_y(mat, 1, True, axis)
-            w_forward(mat, 2, axis)
-    rs_step(2, 5)
-    rs_step(3, 5)
-    rs_step(4, 5)
-    rs_step(5, 5)
-    tap_step(5)
-    for step in range(3):
-        for p in range(6):
-            ag_step(p, step)
-    w_done(1)
-    back(1)
-    w_done(3)
-    back(3)
-    finish(1)
-    finish(3)
-    for p in range(6):
-        ag_step(p, 3)
+    run = {
+        START: start, ELEM: elementwise, TURN: turn, PROD: product, RS: rs_step, AG: ag_step,
+        WY: wy_step, WF: wf_step, TAP: tap_step, BACK: back, FIN: finish,
+    }
+    for op, *numbers in SCHEDULE:
+        with jax.named_scope("_".join(str(n) for n in [NAMES[op]] + numbers)):
+            run[op](*numbers)
     store(stage_g, gwg_hbm)
     store(stage_u, gwu_hbm)
-    w_done(2)
-    back(2)
     tap_copy(6).wait_recv()
     tap_out[tp] = tap[6]
     tap_out[1 - tp] = tap_in[6]
     store(tap_out, taps_hbm)
-    finish(2)
     for copy in pending:
         copy.wait_send()
     for copy in outs:
@@ -417,7 +394,7 @@
 
 
 def fused(x, gate, up, cot, wg, wu, kg, ku):
-    sizes = [GROUPS[group][1] for group, _ in PORTIONS]
+    sizes = [GROUPS[group][1] for group, _, _ in PORTIONS]
     any_space = pl.BlockSpec(memory_space=pl.ANY)
     in_vmem = pl.BlockSpec(memory_space=pltpu.VMEM)
     dma = pltpu.SemaphoreType.DMA
@@ -440,9 +417,9 @@
             pltpu.VMEM((4, 4, 2, 64, FC), BF16),
             pltpu.VMEM((4, 4, 2, 64, FC), BF16),
         ]
-        + [pltpu.VMEM((64, SUB, size), BF16) for size in sizes]
-        + [pltpu.VMEM((63, SUB, size), BF16) for size in sizes]
-        + [pltpu.VMEM((16, SUB, size), BF16) for size in sizes]
+        + [pltpu.VMEM((64, ROWS, size), BF16) for size in sizes]
+        + [pltpu.VMEM((63, ROWS, size), BF16) for size in sizes]
+        + [pltpu.VMEM((16, ROWS, size), BF16) for size in sizes]
         + [
             pltpu.VMEM((512, FC), BF16),
             pltpu.VMEM((512, FC), BF16),
@@ -451,8 +428,8 @@
             pltpu.VMEM((2, 8, FC), F32),
             pltpu.VMEM((4, 2, HALF, 512), BF16),
             pltpu.VMEM((4, HALF, 512), BF16),
-            dma((12,)), dma((36,)), dma((36,)), dma((24,)), dma((24,)),
-            dma((12,)), dma((12,)), dma((24,)), dma((24,)),
+            dma((12,)), dma((6 * COUNT,)), dma((6 * COUNT,)), dma((4 * COUNT,)), dma((4 * COUNT,)),
+            dma((24,)), dma((24,)), dma((24,)), dma((24,)),
             dma((7,)), dma((7,)), dma((1,)), dma((1,)), dma((4,)), dma((4,)), dma((7,)),
         ],
         compiler_params=pltpu.CompilerParams(

time: 150 us -> 124 us (0.83)
  Pallas kernels: 141 us -> 116 us
    pallas_call x1, Pallas kernels: 141 us -> 116 us  [fused(): pl.pallas_call(kernel, in_specs=[any_space] * 6 + [in_vmem] * 2, out_spec...]
where the time goes in v1:
time: 124 us
  Pallas kernels  116 us (94%)
  other arithmetic  4.96 us (4%)
  local copies, waits for them, and re-layouts  2.62 us (2%)
    pallas_call x1, Pallas kernels, fused(): pl.pallas_call(kernel, in_specs=[any_space] * 6 + [in_vmem] * 2, out_spec...  116 us
    mul x1, other arithmetic, per_device(): grad_up.astype(F32) * factor  4.95 us

profile of v1, /device:TPU:1, one launch (start us, length us, event | category | flops | bytes accessed | tf_op | source)
XLA Modules:
  0.0 123.9 jit_solution(3044317500629306982)
XLA Ops:
  0.6 115.7 %shard_map.119 = (bf16[384,2048]{1,0:T(8,128)(2,1)}, bf16[512,1408]{1,0:T(8,128)(2,1)}, bf16[512,1408]{1,0:T(8,128)(2,1)}, f32[2,8,1408]{2,1,0:T(8,128)}) custom-call(bf16[384,2048]{1,0:T(8,128)(2,1)} %bitcast.15, bf16[768,1408]{1,0:T(8,128)(2,1)} %bitcast.12, bf16[768,1408]{1,0:T(8,128)(2,1)} %bitcast.13, bf16[768,1408]{1,0:T(8,128)(2,1)} %bitcast.14, ...), custom_call_target="tpu_custom_call" | custom-call | flops 17999998976 | bytes 20971520 | tf_op jit(solution)/shard_map/pallas_call | solution.py:401
  116.3 0.8 slice_bitcast_fusion.1
  117.2 0.7 fusion
  117.8 0.0 copy-start
  117.8 5.0 %convert_multiply_fusion = (f32[512,1408]{1,0:T(8,128)}, f32[512,1408]{1,0:T(8,128)}) fusion(bf16[512,1408]{1,0:T(8,128)(2,1)} %get-tuple-element.11, bf16[512,1408]{1,0:T(8,128)(2,1)} %get-tuple-element.10), kind=kLoop, calls=%fused_computation | loop fusion | flops 2883584 | bytes 8650752 | tf_op jit(solution)/shard_map/mul | solution.py:453
  122.8 0.0 copy-done
  122.8 1.1 copy.14
  (1 shorter events, 0.0 us)
Async XLA Ops:
  117.8 5.0 %copy-start = (bf16[384,2048]{1,0:T(8,128)(2,1)S(1)}, bf16[384,2048]{1,0:T(8,128)(2,1)}, u32[]{:S(2)}) copy-start(bf16[384,2048]{1,0:T(8,128)(2,1)} %get-tuple-element.9) | copy-start | bytes 4718596

commit v2 on v1

v2 whole, which is shorter than its diff:
```python
import functools

import jax
import jax.numpy as jnp
from jax import lax
from jax.experimental import pallas as pl
from jax.experimental.pallas import tpu as pltpu
from jax.sharding import PartitionSpec as P

F32 = jnp.float32
BF16 = jnp.bfloat16
MESH = pl.DeviceIdType.MESH

Y1, Y3, X1, X3, Z1, Z3 = range(6)
CYCLE = (X1, Z1, X3, Z3, Y1, Y3)
REP_CYCLE = (X1, Z1, X3, Z3)
GROUPS = ((0, 512), (512, 512), (1024, 384))
SPLIT = 2
SUB = 32
ROWS = SUB // SPLIT
PORTIONS = tuple((group, mat, h) for group in range(len(GROUPS)) for mat in range(2) for h in range(SPLIT))
COUNT = len(PORTIONS)
GROUP_ORDER = (0, 1, 2)
ORDERS = (
    (Z1, X1, X3, Y1, Z3, Y3), (Z3, X1, Y1, Y3, Z1, X3), (X1, Y3, Z3, Z1, X3, Y1), (X3, Z3, Z1, Y1, X1, Y3),
    (Y1, X1, Z1, Z3, Y3, X3), (X3, Z3, X1, Y1, Y3, Z1), (Z3, X3, Z1, Y3, Y1, X1), (X1, Y3, X3, Z1, Z3, Y1),
    (Z3, Z1, X1, Y3, X3, Y1), (Z1, X3, X1, Z3, Y3, Y1), (Y1, Z1, X3, X1, Y3, Z3), (Y3, Z1, X3, Z3, X1, Y1),
)
AG_ORDERS = (
    (X3, Z1, X1, Z3), (Z1, Z3, X3, X1), (X3, X1, Z3, Z1), (Z1, Z3, X3, X1), (Z3, X1, Z1, X3),
    (Z3, X3, X1, Z1), (Z3, X3, Z1, X1), (Z1, Z3, X1, X3), (X1, X3, Z1, Z3), (X1, Z1, Z3, X3),
    (Z1, X1, X3, Z3), (Z3, X3, X1, Z1),
)
DIRECT = ((0, 0), (1, 3))
LEN = 768
HALF = 384
D = 2048
FC = 1408
STEP = 1024
W_PATHS = ((Y1, Y3), (Y3, Y1))
MASK = {Y1: 1, Y3: 3}


def recv_offset(stage):
    return 64 - 2 ** (6 - stage)


START, ELEM, TURN, PROD, RS, AG, WY, WF, TAP, BACK, FIN = range(11)
NAMES = ("start", "elem", "turn", "prod", "rs", "ag", "wy", "wf", "tap", "back", "fin")
SCHEDULE = (
    (ELEM, 0, 0, 1), (TURN, 0), (START,), (WY, 0, 0, Y1, 2, 0), (WY, 1, 0, Y3, 1, 0), (ELEM, 0, 1, 4),
    (WY, 0, 0, Y1, 0, 0), (WY, 0, 0, Y3, 2, 0), (TURN, 1), (PROD, 0, 0), (WY, 0, 0, Y1, 3, 0),
    (WY, 1, 0, Y3, 3, 0), (WF, 1, 3, 1), (PROD, 0, 1), (ELEM, 1, 0, 2), (WY, 1, 0, Y1, 0, 0),
    (WY, 1, 0, Y3, 0, 0), (ELEM, 1, 2, 4), (PROD, 1, 0), (WY, 0, 0, Y3, 1, 0), (PROD, 1, 1), (ELEM, 2, 0, 1),
    (WF, 0, 1, 2), (ELEM, 2, 1, 3), (WY, 0, 0, Y3, 0, 0), (PROD, 2, 0), (TAP, -1), (PROD, 2, 1), (RS, 0, 0),
    (RS, 2, 0), (RS, 1, 0), (BACK, 0, 0), (RS, 3, 0), (BACK, 0, 1), (FIN, 0, 0), (FIN, 0, 1), (RS, 4, 0),
    (WF, 0, 3, 2), (RS, 6, 0), (RS, 9, 0), (TAP, 0), (RS, 7, 0), (RS, 11, 0), (WY, 1, 0, Y1, 1, 0),
    (RS, 5, 0), (RS, 10, 0), (WY, 0, 0, Y1, 1, 0), (RS, 0, 1), (RS, 2, 1), (RS, 8, 0), (RS, 11, 1),
    (RS, 6, 1), (WY, 1, 0, Y1, 2, 0), (WY, 1, 0, Y3, 2, 0), (TAP, 1), (RS, 1, 1), (RS, 10, 1), (RS, 9, 1),
    (RS, 3, 1), (RS, 7, 1), (WY, 0, 1, Y3, 1, 0), (RS, 0, 2), (RS, 8, 1), (RS, 11, 2), (RS, 4, 1),
    (WY, 1, 0, Y1, 3, 0), (WY, 0, 1, Y3, 2, 0), (RS, 5, 1), (WF, 0, 1, 3), (WF, 0, 1, 1), (RS, 6, 2),
    (RS, 10, 2), (RS, 1, 2), (RS, 9, 2), (RS, 0, 3), (RS, 2, 2), (TAP, 2), (WY, 1, 3, Y1, 0, 0), (RS, 3, 2),
    (RS, 11, 3), (RS, 7, 2), (RS, 8, 2), (WF, 0, 3, 1), (WF, 1, 3, 0), (WF, 1, 3, 2), (RS, 4, 2), (RS, 5, 2),
    (WY, 0, 0, Y3, 3, 0), (RS, 2, 3), (RS, 6, 3), (RS, 10, 3), (RS, 11, 4), (RS, 9, 3), (RS, 7, 3),
    (WF, 1, 1, 0), (RS, 0, 4), (RS, 1, 3), (WF, 0, 2, 1), (RS, 8, 3), (WF, 1, 1, 2), (RS, 4, 3),
    (WY, 1, 3, Y1, 1, 0), (TAP, 3), (RS, 3, 3), (RS, 7, 4), (RS, 5, 3), (RS, 2, 4), (RS, 1, 4), (RS, 6, 4),
    (WY, 0, 1, Y3, 0, 0), (RS, 11, 5), (WF, 1, 2, 0), (WF, 0, 3, 3), (WF, 1, 1, 1), (RS, 10, 4),
    (WF, 0, 2, 2), (RS, 9, 4), (RS, 0, 5), (WY, 1, 3, Y1, 2, 0), (RS, 4, 4), (AG, 11, 0), (RS, 3, 4),
    (RS, 5, 4), (RS, 6, 5), (RS, 8, 4), (RS, 1, 5), (WY, 0, 1, Y3, 3, 0), (RS, 7, 5), (RS, 2, 5), (RS, 9, 5),
    (WY, 1, 3, Y1, 3, 0), (WF, 1, 2, 1), (RS, 10, 5), (AG, 6, 0), (RS, 3, 5), (TAP, 4), (AG, 9, 0),
    (WY, 1, 0, Y3, 3, 1), (AG, 0, 0), (RS, 4, 5), (RS, 5, 5), (WF, 1, 2, 2), (AG, 11, 1), (RS, 8, 5),
    (AG, 1, 0), (AG, 2, 0), (AG, 7, 0), (AG, 10, 0), (WY, 0, 0, Y1, 0, 1), (AG, 3, 0), (AG, 9, 1), (AG, 4, 0),
    (AG, 0, 1), (WF, 0, 2, 3), (AG, 5, 0), (WY, 0, 0, Y3, 0, 1), (AG, 1, 1), (AG, 11, 2), (AG, 8, 0),
    (AG, 7, 1), (AG, 2, 1), (AG, 3, 1), (WY, 1, 0, Y1, 3, 1), (TAP, 5), (AG, 10, 1), (AG, 6, 1), (AG, 4, 1),
    (AG, 5, 1), (AG, 9, 2), (BACK, 3, 1), (AG, 0, 2), (AG, 1, 2), (AG, 8, 1), (WY, 0, 1, Y3, 0, 1),
    (BACK, 1, 0), (WY, 1, 3, Y1, 3, 1), (AG, 7, 2), (AG, 3, 2), (FIN, 3, 1), (AG, 11, 3), (AG, 6, 2),
    (AG, 5, 2), (BACK, 3, 0), (AG, 2, 2), (AG, 4, 2), (AG, 10, 2), (FIN, 1, 0), (BACK, 1, 1), (AG, 8, 2),
    (AG, 9, 3), (AG, 1, 3), (FIN, 3, 0), (AG, 0, 3), (BACK, 2, 0), (AG, 7, 3), (AG, 5, 3), (FIN, 1, 1),
    (AG, 3, 3), (BACK, 2, 1), (AG, 10, 3), (FIN, 2, 0), (AG, 4, 3), (AG, 2, 3), (AG, 8, 3), (AG, 6, 3),
    (FIN, 2, 1),
)


def kernel(
    x_hbm, gate_hbm, up_hbm, cot_hbm, wg_hbm, wu_hbm, kg_ref, ku_ref,
    gin_hbm, taps_hbm, *rest,
):
    sums, (xs, xt, act_g, act_u, act_c, ws_g, ws_u, *scratch) = rest[:COUNT], rest[COUNT:]
    gs, rs, ags = (scratch[i * COUNT : (i + 1) * COUNT] for i in range(3))
    (
        tap, tap_in, tap_out, part, part_in,
        load_sem, rs_send, rs_recv, ag_send, ag_recv, w_send, wy_recv, wf_recv,
        t_send, t_recv, x_send, x_recv, o_send, o_recv, out_sem, sum_sem,
    ) = scratch[3 * COUNT :]
    ws = (ws_g, ws_u)
    acts = (act_g, act_u)
    rep, y, tp = lax.axis_index("rep"), lax.axis_index("fs"), lax.axis_index("tp")
    z, x = rep // 4, rep % 4

    def gray(c):
        return (c + c // 2) % 2, c // 2

    bits = gray(y) + gray(x) + gray(z)

    def flip1(c):
        return c + 1 - 2 * (c % 2)

    peers = (
        {"fs": flip1(y)}, {"fs": 3 - y},
        {"rep": z * 4 + flip1(x)}, {"rep": z * 4 + 3 - x},
        {"rep": flip1(z) * 4 + x}, {"rep": (3 - z) * 4 + x},
    )
    other_core = {"tp": 1 - tp}

    def remote(src, dst, send, recv, peer):
        return pltpu.make_async_remote_copy(
            src_ref=src, dst_ref=dst, send_sem=send, recv_sem=recv, device_id=peer, device_id_type=MESH
        )

    def send(copy):
        copy.start()

    loads = {}

    def load(name, src, dst):
        copy = pltpu.make_async_copy(src, dst, load_sem.at[len(loads)])
        copy.start()
        loads[name] = copy

    def load_group(key, first, size):
        for name, src, dst in (("g", gate_hbm, act_g), ("u", up_hbm, act_u), ("c", cot_hbm, act_c)):
            load(name + str(key), src.at[:, pl.ds(first, size)], dst.at[:, pl.ds(first, size)])

    barrier = pltpu.get_barrier_semaphore()
    for peer in peers + (other_core,):
        pl.semaphore_signal(barrier, inc=1, device_id=peer, device_id_type=MESH)
    load_group("first", 0, 128)
    load_group(0, 128, GROUPS[0][1] - 128)
    load("x", x_hbm, xs.at[tp])
    for mat, src in enumerate((wg_hbm, wu_hbm)):
        load("w" + str(mat), src, ws[mat].at[0])
    for group in range(1, len(GROUPS)):
        load_group(group, *GROUPS[group])
    tap[0] = jnp.zeros((8, FC), F32)

    parity = (x % 2, z % 2)

    waited = set()

    def wy_copy(mat, src_mask, dim, link, far):
        dst_mask = src_mask ^ MASK[dim]
        at = (mat * 3 + dst_mask - 1) * 4 + link
        half = parity[link // 2]
        if far:
            at, half = 24 + DIRECT.index((mat, link)) * 3 + dst_mask - 1, 1 - half
        return remote(
            ws[mat].at[src_mask, link, half], ws[mat].at[dst_mask, link, half],
            w_send.at[mat], wy_recv.at[at], peers[dim],
        )

    def wf_copy(mat, mask, link):
        half = ws[mat].at[mask, link, parity[link // 2]]
        at = (mask - 1) * 2 + link // 2
        return remote(half, half, w_send.at[mat], wf_recv.at[at], peers[2 + link])

    def landed(ref, sem):
        pltpu.make_async_copy(ref, ref, sem).wait()

    def wf_wait(mask, n):
        count = 4 - sum(link // 2 == n for _, link in DIRECT)
        if count:
            landed(ws[0].at[pl.ds(0, count), 0, 0], wf_recv.at[(mask - 1) * 2 + n])

    def wy_wait(mat, mask, link, far):
        first, second = W_PATHS[mat]
        dim, src = {MASK[first]: (first, 0), MASK[second]: (second, 0), 2: (second, MASK[first])}[mask]
        if (mat, mask, link, far) not in waited:
            waited.add((mat, mask, link, far))
            wy_copy(mat, src, dim, link, far).wait_recv()

    def own_loaded(mat):
        if mat not in waited:
            waited.add(mat)
            loads["w" + str(mat)].wait()

    def wy_step(mat, src_mask, dim, link, far):
        if src_mask:
            wy_wait(mat, src_mask, link, far)
        else:
            own_loaded(mat)
        send(wy_copy(mat, src_mask, dim, link, far))

    def wf_step(mat, mask, link):
        wy_wait(mat, mask, link, 0)
        send(wf_copy(mat, mask, link))

    row = lax.broadcasted_iota(jnp.int32, (8, 128), 0)

    def past(value, steps):
        turned = pltpu.roll(value, steps, 0)
        return jnp.concatenate([jnp.where(row >= steps, turned[:8], 0.0), turned[8:]], axis=0)

    def ahead(value, steps):
        turned = pltpu.roll(value, LEN - steps, 0)
        return jnp.concatenate([turned[:-8], jnp.where(row < 8 - steps, turned[-8:], 0.0)], axis=0)

    def group_loaded(group):
        if ("group", group) not in waited:
            waited.add(("group", group))
            for name in ("g", "u", "c"):
                loads[name + str(group)].wait()

    def elementwise_block(first, j):
        cols = pl.ds(pl.multiple_of(first + j * 128, 128), 128)
        tap_cols = pl.ds(pl.multiple_of(tp * FC + first + j * 128, 128), 128)
        kg_all = kg_ref[:, tap_cols].astype(F32)
        ku_all = ku_ref[:, tap_cols].astype(F32)
        kg = [kg_all[i : i + 1, :] for i in range(3)]
        ku = [ku_all[i : i + 1, :] for i in range(3)]
        gate = act_g[:, cols].astype(F32)
        gates = (past(gate, 2), past(gate, 1), gate)
        mixed_gate = kg[0] * gates[0] + kg[1] * gates[1] + kg[2] * gates[2]
        up = act_u[:, cols].astype(F32)
        ups = (past(up, 2), past(up, 1), up)
        mixed_up = ku[0] * ups[0] + ku[1] * ups[1] + ku[2] * ups[2]
        scale = (2.0 / 3.141592653589793) ** 0.5
        square = mixed_gate * mixed_gate
        bent = jnp.tanh(mixed_gate * (scale + (scale * 0.044715) * square))
        lift = 0.5 + 0.5 * bent
        slope = lift + mixed_gate * (1.0 - bent * bent) * (0.5 * scale + (1.5 * 0.044715 * scale) * square)
        cot = act_c[:, cols].astype(F32)
        back_up = cot * (mixed_gate * lift)
        back_gate = cot * mixed_up * slope
        dg = kg[2] * back_gate + kg[1] * ahead(back_gate, 1) + kg[0] * ahead(back_gate, 2)
        du = ku[2] * back_up + ku[1] * ahead(back_up, 1) + ku[0] * ahead(back_up, 2)
        act_g[:, cols] = dg.astype(BF16)
        act_u[:, cols] = du.astype(BF16)
        for i in range(3):
            tap[0, pl.ds(i, 1), cols] = jnp.sum(back_gate * gates[i], axis=0, keepdims=True)
            tap[0, pl.ds(3 + i, 1), cols] = jnp.sum(back_up * ups[i], axis=0, keepdims=True)

    def elementwise(group, begin, end):
        if group == 0 and begin == 0:
            group_loaded("first")
            elementwise_block(0, 0)
            begin = 1
        group_loaded(group)

        def block(j, _):
            elementwise_block(GROUPS[group][0], j)
            return 0

        lax.fori_loop(begin, end, block, 0)

    def product_block(group, mat, step):
        first, size = GROUPS[group]
        value = jnp.dot(
            xt[pl.ds(pl.multiple_of(step * STEP, STEP), STEP), :],
            acts[mat][:, pl.ds(first, size)],
            preferred_element_type=F32,
        ).astype(BF16)
        for k in range(STEP // 512):
            low, high = gray(step * (STEP // 512) + k)
            for p in range(COUNT):
                if PORTIONS[p][:2] != (group, mat):
                    continue
                place = {ORDERS[p][s]: 2 ** (5 - s) for s in range(6)}
                base = low * place[Y1] + high * place[Y3]
                for sub in range(16):
                    at = sum(((sub >> i) & 1) * place[2 + i] for i in range(4))
                    row_at = k * 512 + sub * SUB + PORTIONS[p][2] * ROWS
                    gs[p][base + at] = value[row_at : row_at + ROWS, :]

    def product_done(group, mat):
        for p in range(COUNT):
            if PORTIONS[p][:2] == (group, mat):
                send(rs_copy(p, 0))

    def product(group, mat):
        def block(step, _):
            product_block(group, mat, step)
            return 0

        lax.fori_loop(0, D // STEP, block, 0)
        product_done(group, mat)

    def base_of(p, stage):
        return sum(bits[ORDERS[p][s]] * 2 ** (5 - s) for s in range(stage))

    def rs_copy(p, stage):
        dim, count = ORDERS[p][stage], 2 ** (5 - stage)
        start = base_of(p, stage) + (1 - bits[dim]) * count
        at = p * 6 + stage
        return remote(
            gs[p].at[pl.ds(start, count)], rs[p].at[pl.ds(recv_offset(stage), count)],
            rs_send.at[p], rs_recv.at[at], peers[dim],
        )

    def ag_at(p):
        return sum(bits[dim] * 2**t for t, dim in enumerate(AG_ORDERS[p]))

    def ag_copy(p, step):
        count = 2**step
        held = ags[p].at[pl.ds((ag_at(p) // count) * count, count)]
        at = p * 4 + step
        return remote(held, held, ag_send.at[p], ag_recv.at[at], peers[AG_ORDERS[p][step]])

    def rs_step(p, stage):
        rs_copy(p, stage).wait_recv()
        start, count, offset = base_of(p, stage + 1), 2 ** (5 - stage), recv_offset(stage)

        def total(i):
            return (gs[p][start + i].astype(F32) + rs[p][offset + i].astype(F32)).astype(BF16)

        if stage == 5:
            ags[p][ag_at(p)] = total(0)
            send(ag_copy(p, 0))
            return

        def add(i, _):
            gs[p][start + i] = total(i)
            return 0

        lax.fori_loop(0, count, add, 0)
        send(rs_copy(p, stage + 1))

    def ag_step(p, step):
        ag_copy(p, step).wait_recv()
        if step < 3:
            send(ag_copy(p, step + 1))
            return
        pltpu.make_async_copy(ags[p], sums[p], sum_sem.at[PORTIONS[p][0]]).start()

    def tap_copy(step):
        peer = peers[step] if step < 6 else other_core
        return remote(tap.at[step], tap_in.at[step], t_send.at[0], t_recv.at[step], peer)

    def tap_step(step):
        if step >= 0:
            tap_copy(step).wait_recv()
            tap[step + 1] = tap[step] + tap_in[step]
        send(tap_copy(step + 1))

    def back(mask, n):
        for mat in range(2):
            own_loaded(mat)
            for link in (2 * n, 2 * n + 1) if mask else ():
                wy_wait(mat, mask, link, 0)
                if (mat, link) in DIRECT:
                    wy_wait(mat, mask, link, 1)
        if mask:
            wf_wait(mask, n)

        def dot(mat):
            weights = ws[mat][mask, pl.ds(2 * n, 2)].reshape(256, FC)
            return lax.dot_general(
                acts[mat][...], weights, (((1,), (1,)), ((), ())), preferred_element_type=F32
            )

        value = (dot(0) + dot(1)).astype(BF16)
        part[mask, n, 0] = value[:HALF]
        part[mask, n, 1] = value[HALF:]
        send(part_copy(mask, n))

    def part_copy(mask, n):
        return remote(
            part.at[mask, n, 1 - tp], part_in.at[mask, n], o_send.at[0], o_recv.at[mask * 2 + n], other_core
        )

    def finish(mask, n):
        part_copy(mask, n).wait_recv()
        part_in[mask, n] = (part[mask, n, tp].astype(F32) + part_in[mask, n].astype(F32)).astype(BF16)
        block = {0: y, 1: flip1(y), 2: (y + 2) % 4, 3: 3 - y}[mask]
        cols = pl.ds(pl.multiple_of(block * 512 + n * 256, 256), 256)
        pltpu.make_async_copy(part_in.at[mask, n], gin_hbm.at[:, cols], out_sem.at[0]).start()

    def x_loaded():
        if "x" not in waited:
            waited.add("x")
            loads["x"].wait()

    def turn(second):
        if second:
            x_copy.wait_recv()
        else:
            x_loaded()
        which = 1 - tp if second else tp
        rows = pl.ds(pl.multiple_of(which * HALF, HALF), HALF)

        def block(c, _):
            cols = pl.ds(pl.multiple_of(c * 128, 128), 128)
            xt[cols, rows] = xs[which, :, cols].T
            return 0

        lax.fori_loop(0, D // 128, block, 0)

    def start():
        pl.semaphore_wait(barrier, 7)
        x_loaded()
        send(x_copy)

    x_copy = remote(xs.at[tp], xs.at[tp], x_send.at[0], x_recv.at[0], other_core)
    run = {
        START: start, ELEM: elementwise, TURN: turn, PROD: product, RS: rs_step, AG: ag_step,
        WY: wy_step, WF: wf_step, TAP: tap_step, BACK: back, FIN: finish,
    }
    for op, *numbers in SCHEDULE:
        with jax.named_scope("_".join(str(n) for n in [NAMES[op]] + numbers)):
            run[op](*numbers)
    with jax.named_scope("tail_taps"):
        tap_copy(6).wait_recv()
        tap_out[tp] = tap[6]
        tap_out[1 - tp] = tap_in[6]
        tap_store = pltpu.make_async_copy(tap_out, taps_hbm, out_sem.at[1])
        tap_store.start()
    with jax.named_scope("tail_sends"):
        for p in range(COUNT):
            landed(rs[p], rs_send.at[p])
            landed(ags[p].at[pl.ds(0, 15)], ag_send.at[p])
        for mat in range(2):
            landed(ws[mat].at[pl.ds(0, 3)], w_send.at[mat])
        landed(tap, t_send.at[0])
        landed(part_in, o_send.at[0])
        x_copy.wait_send()
    with jax.named_scope("tail_stores"):
        for group in range(len(GROUPS)):
            landed(gs[group * 2 * SPLIT].at[pl.ds(0, 32 * SPLIT)], sum_sem.at[group])
        landed(part_in, out_sem.at[0])
        tap_store.wait()


def fused(x, gate, up, cot, wg, wu, kg, ku):
    sizes = [GROUPS[group][1] for group, _, _ in PORTIONS]
    any_space = pl.BlockSpec(memory_space=pl.ANY)
    in_vmem = pl.BlockSpec(memory_space=pltpu.VMEM)
    dma = pltpu.SemaphoreType.DMA
    return pl.pallas_call(
        kernel,
        in_specs=[any_space] * 6 + [in_vmem] * 2,
        out_specs=[any_space] * (2 + COUNT),
        out_shape=[jax.ShapeDtypeStruct((HALF, D), BF16), jax.ShapeDtypeStruct((2, 8, FC), F32)]
        + [jax.ShapeDtypeStruct((16, ROWS, size), BF16) for size in sizes],
        scratch_shapes=[
            pltpu.VMEM((2, HALF, D), BF16),
            pltpu.VMEM((D, LEN), BF16),
            pltpu.VMEM((LEN, FC), BF16),
            pltpu.VMEM((LEN, FC), BF16),
            pltpu.VMEM((LEN, FC), BF16),
            pltpu.VMEM((4, 4, 2, 64, FC), BF16),
            pltpu.VMEM((4, 4, 2, 64, FC), BF16),
        ]
        + [pltpu.VMEM((64, ROWS, size), BF16) for size in sizes]
        + [pltpu.VMEM((63, ROWS, size), BF16) for size in sizes]
        + [pltpu.VMEM((16, ROWS, size), BF16) for size in sizes]
        + [
            pltpu.VMEM((7, 8, FC), F32),
            pltpu.VMEM((7, 8, FC), F32),
            pltpu.VMEM((2, 8, FC), F32),
            pltpu.VMEM((4, 2, 2, HALF, 256), BF16),
            pltpu.VMEM((4, 2, HALF, 256), BF16),
            dma((6 + 3 * len(GROUPS),)),
            dma((COUNT,)), dma((6 * COUNT,)), dma((COUNT,)), dma((4 * COUNT,)),
            dma((2,)), dma((24 + 3 * len(DIRECT),)), dma((6,)),
            dma((1,)), dma((7,)), dma((1,)), dma((1,)), dma((1,)), dma((8,)), dma((2,)), dma((len(GROUPS),)),
        ],
        compiler_params=pltpu.CompilerParams(
            collective_id=0, has_side_effects=True, vmem_limit_bytes=67043328
        ),
        cost_estimate=pl.CostEstimate(flops=18 * 10**9, bytes_accessed=20 * 2**20, transcendentals=10**6),
    )(x, gate, up, cot, wg, wu, kg, ku)


def finish_kernel(factor, gin_hbm, taps_ref, *rest):
    sums, rest = rest[:COUNT], rest[COUNT:]
    gin_out, gate_out, up_out, tap_gate, tap_up, gin, *rest = rest
    held, (wide_gate, wide_up, in_sem, out_sem) = rest[:COUNT], rest[COUNT:]
    wide, results = (wide_gate, wide_up), (gate_out, up_out)
    copies = [pltpu.make_async_copy(sums[p], held[p], in_sem.at[p]) for p in range(COUNT)]
    for copy in copies:
        copy.start()
    gin_in = pltpu.make_async_copy(gin_hbm, gin, in_sem.at[COUNT])
    gin_in.start()
    for i in range(2):
        cols = pl.ds(i * FC, FC)
        tap_gate[:, cols] = factor * taps_ref[i, :3, :]
        tap_up[:, cols] = factor * taps_ref[i, 3:6, :]
    outs = []
    for p in range(COUNT):
        with jax.named_scope("sum_wait_" + str(p)):
            copies[p].wait()
        group, mat, h = PORTIONS[p]
        first, size = GROUPS[group]
        for sub in range(16):
            at = sum(((sub >> (dim - 2)) & 1) * 2**t for t, dim in enumerate(AG_ORDERS[p]))
            rows = pl.ds(sub * SUB + h * ROWS, ROWS)
            wide[mat][rows, pl.ds(first, size)] = factor * held[p][at].astype(F32)
        if h == SPLIT - 1:
            cols = pl.ds(first, size)
            copy = pltpu.make_async_copy(wide[mat].at[:, cols], results[mat].at[:, cols], out_sem.at[len(outs)])
            copy.start()
            outs.append(copy)
    gin_in.wait()
    copy = pltpu.make_async_copy(gin, gin_out, out_sem.at[len(outs)])
    copy.start()
    with jax.named_scope("last_wait"):
        for copy in outs + [copy]:
            copy.wait()


def finished(factor, gin, taps, sums):
    any_space = pl.BlockSpec(memory_space=pl.ANY)
    in_vmem = pl.BlockSpec(memory_space=pltpu.VMEM)
    return pl.pallas_call(
        functools.partial(finish_kernel, factor),
        in_specs=[any_space, in_vmem] + [any_space] * COUNT,
        out_specs=[any_space] * 3 + [in_vmem] * 2,
        out_shape=[
            jax.ShapeDtypeStruct((HALF, D), BF16),
            jax.ShapeDtypeStruct((512, FC), F32),
            jax.ShapeDtypeStruct((512, FC), F32),
            jax.ShapeDtypeStruct((3, 2 * FC), F32),
            jax.ShapeDtypeStruct((3, 2 * FC), F32),
        ],
        scratch_shapes=[pltpu.VMEM((HALF, D), BF16)]
        + [pltpu.VMEM(part.shape, BF16) for part in sums]
        + [
            pltpu.VMEM((512, FC), F32),
            pltpu.VMEM((512, FC), F32),
            pltpu.SemaphoreType.DMA((COUNT + 1,)),
            pltpu.SemaphoreType.DMA((COUNT + 1,)),
        ],
        compiler_params=pltpu.CompilerParams(vmem_limit_bytes=60 * 2**20),
    )(gin, taps, *sums)


def per_device(inputs, pre_gate, pre_up, cotangent, w_gate, w_up, taps_gate, taps_up):
    count = LEN * lax.axis_size("rep") * lax.axis_size("fs")
    factor = float(count) ** (-0.5)
    grad_inputs, taps, *sums = fused(
        inputs[0], pre_gate[0], pre_up[0], cotangent[0],
        w_gate.reshape(4, 2, 64, FC), w_up.reshape(4, 2, 64, FC), taps_gate, taps_up,
    )
    grad_inputs, grad_gate, grad_up, grad_taps_gate, grad_taps_up = finished(factor, grad_inputs, taps, sums)
    return grad_inputs[None], grad_gate, grad_up, grad_taps_gate, grad_taps_up


def solution(mesh):
    placed = (
        P(("rep", "fs"), "tp", None),
        P(("rep", "fs"), None, "tp"),
        P(("rep", "fs"), None, "tp"),
        P(("rep", "fs"), None, "tp"),
        P("fs", "tp"),
        P("fs", "tp"),
        P(),
        P(),
    )
    return jax.shard_map(
        per_device,
        mesh=mesh,
        in_specs=placed,
        out_specs=(P(("rep", "fs"), "tp", None), P("fs", "tp"), P("fs", "tp"), P(), P()),
        check_vma=False,
    )
```

time: 124 us -> 119 us (0.960)
  other arithmetic: 4.96 us -> 0 us
  local copies, waits for them, and re-layouts: 2.62 us -> 0 us
  Pallas kernels: 116 us -> 118 us
    pallas_call x0 -> x1, Pallas kernels: none -> 5.83 us  [finished(): pl.pallas_call(functools.partial(finish_kernel, factor), in_specs=[any_sp...]
    mul x2 -> x0, other arithmetic: 4.96 us -> none  [the longest x1 4.95 us: per_device(): grad_up.astype(F32) * factor]
    pallas_call x1, Pallas kernels: 116 us -> 113 us  [fused(): pl.pallas_call(kernel, in_specs=[any_space] * 6 + [in_vmem] * 2, out_spec...]
where the time goes in v2:
time: 119 us
  Pallas kernels  118 us (99%)
    pallas_call x1, Pallas kernels, fused(): pl.pallas_call(kernel, in_specs=[any_space] * 6 + [in_vmem] * 2, out_spec...  113 us
    pallas_call x1, Pallas kernels, finished(): pl.pallas_call(functools.partial(finish_kernel, factor), in_specs=[any_sp...  5.83 us

profile of v2, /device:TPU:1, one launch (start us, length us, event | category | flops | bytes accessed | tf_op | source)
XLA Modules:
  0.0 119.3 jit_solution(8020969321676545837)
XLA Ops:
  0.6 112.6 %shard_map.119 = (bf16[384,2048]{1,0:T(8,128)(2,1)}, f32[2,8,1408]{2,1,0:T(8,128)}, bf16[16,16,512]{2,1,0:T(8,128)(2,1)}, bf16[16,16,512]{2,1,0:T(8,128)(2,1)}, ...) custom-call(bf16[384,2048]{1,0:T(8,128)(2,1)} %bitcast.10, ...), custom_call_target="tpu_custom_call" | custom-call | flops 17999998976 | bytes 20971520 | tf_op jit(solution)/shard_map/pallas_call | solution.py:437
  113.3 5.8 %shard_map.120 = (bf16[384,2048]{1,0:T(8,128)(2,1)}, f32[512,1408]{1,0:T(8,128)}, f32[512,1408]{1,0:T(8,128)}, f32[3,2816]{1,0:T(4,128)}, f32[3,2816]{1,0:T(4,128)}) custom-call(bf16[384,2048]{1,0:T(8,128)(2,1)} %get-tuple-element.24.gin_hbm, f32[2,8,1408]{2,1,0:T(8,128)} %get-tuple-element.25.taps_ref, bf16[16,16,512]{2,1,0:T(8,128)(2,1)} %get-tuple-element.26.rest_0_, ...), custom_call_target="tpu_custom_call" | custom-call | tf_op jit(solution)/shard_map/pallas_call | solution.py:513

commit v3 on v2

--- a/solution.py
+++ b/solution.py
@@ -351,15 +351,19 @@
         if mask:
             wf_wait(mask, n)
 
-        def dot(mat):
-            weights = ws[mat][mask, pl.ds(2 * n, 2)].reshape(256, FC)
-            return lax.dot_general(
-                acts[mat][...], weights, (((1,), (1,)), ((), ())), preferred_element_type=F32
-            )
-
-        value = (dot(0) + dot(1)).astype(BF16)
-        part[mask, n, 0] = value[:HALF]
-        part[mask, n, 1] = value[HALF:]
+        def block(k, _):
+            def dot(mat):
+                weights = ws[mat][mask, pl.ds(2 * k, 2)].reshape(256, FC)
+                return lax.dot_general(
+                    acts[mat][...], weights, (((1,), (1,)), ((), ())), preferred_element_type=F32
+                )
+
+            value = (dot(0) + dot(1)).astype(BF16)
+            part[mask, k, 0] = value[:HALF]
+            part[mask, k, 1] = value[HALF:]
+            return 0
+
+        lax.fori_loop(n, n + 1 + (tp // 2), block, 0)
         send(part_copy(mask, n))
 
     def part_copy(mask, n):
@@ -475,16 +479,18 @@
     gin_out, gate_out, up_out, tap_gate, tap_up, gin, *rest = rest
     held, (wide_gate, wide_up, in_sem, out_sem) = rest[:COUNT], rest[COUNT:]
     wide, results = (wide_gate, wide_up), (gate_out, up_out)
+    gin_in = pltpu.make_async_copy(gin_hbm, gin, in_sem.at[COUNT])
+    gin_in.start()
     copies = [pltpu.make_async_copy(sums[p], held[p], in_sem.at[p]) for p in range(COUNT)]
     for copy in copies:
         copy.start()
-    gin_in = pltpu.make_async_copy(gin_hbm, gin, in_sem.at[COUNT])
-    gin_in.start()
     for i in range(2):
         cols = pl.ds(i * FC, FC)
         tap_gate[:, cols] = factor * taps_ref[i, :3, :]
         tap_up[:, cols] = factor * taps_ref[i, 3:6, :]
-    outs = []
+    gin_in.wait()
+    outs = [pltpu.make_async_copy(gin, gin_out, out_sem.at[0])]
+    outs[0].start()
     for p in range(COUNT):
         with jax.named_scope("sum_wait_" + str(p)):
             copies[p].wait()
@@ -499,11 +505,8 @@
             copy = pltpu.make_async_copy(wide[mat].at[:, cols], results[mat].at[:, cols], out_sem.at[len(outs)])
             copy.start()
             outs.append(copy)
-    gin_in.wait()
-    copy = pltpu.make_async_copy(gin, gin_out, out_sem.at[len(outs)])
-    copy.start()
     with jax.named_scope("last_wait"):
-        for copy in outs + [copy]:
+        for copy in outs:
             copy.wait()
 
 

time: 119 us -> 114 us (0.958)
  Pallas kernels: 118 us -> 113 us
    pallas_call x1, Pallas kernels: 113 us -> 107 us  [fused(): pl.pallas_call(kernel, in_specs=[any_space] * 6 + [in_vmem] * 2, out_spec...]
where the time goes in v3:
time: 114 us
  Pallas kernels  113 us (99%)
    pallas_call x1, Pallas kernels, fused(): pl.pallas_call(kernel, in_specs=[any_space] * 6 + [in_vmem] * 2, out_spec...  107 us
    pallas_call x1, Pallas kernels, finished(): pl.pallas_call(functools.partial(finish_kernel, factor), in_specs=[any_sp...  6.16 us

profile of v3, /device:TPU:1, one launch (start us, length us, event | category | flops | bytes accessed | tf_op | source)
XLA Modules:
  0.0 113.6 jit_solution(3033743609031945453)
XLA Ops:
  0.6 106.6 %shard_map.119 = (bf16[384,2048]{1,0:T(8,128)(2,1)}, f32[2,8,1408]{2,1,0:T(8,128)}, bf16[16,16,512]{2,1,0:T(8,128)(2,1)}, bf16[16,16,512]{2,1,0:T(8,128)(2,1)}, ...) custom-call(bf16[384,2048]{1,0:T(8,128)(2,1)} %bitcast.10, ...), custom_call_target="tpu_custom_call" | custom-call | flops 17999998976 | bytes 20971520 | tf_op jit(solution)/shard_map/pallas_call | solution.py:441
  107.3 6.2 %shard_map.120 = (bf16[384,2048]{1,0:T(8,128)(2,1)}, f32[512,1408]{1,0:T(8,128)}, f32[512,1408]{1,0:T(8,128)}, f32[3,2816]{1,0:T(4,128)}, f32[3,2816]{1,0:T(4,128)}) custom-call(bf16[384,2048]{1,0:T(8,128)(2,1)} %get-tuple-element.24.gin_hbm, f32[2,8,1408]{2,1,0:T(8,128)} %get-tuple-element.25.taps_ref, bf16[16,16,512]{2,1,0:T(8,128)(2,1)} %get-tuple-element.26.rest_0_, ...), custom_call_target="tpu_custom_call" | custom-call | tf_op jit(solution)/shard_map/pallas_call | solution.py:516

commit v4 on v3

--- a/solution.py
+++ b/solution.py
@@ -22,16 +22,16 @@
 COUNT = len(PORTIONS)
 GROUP_ORDER = (0, 1, 2)
 ORDERS = (
-    (Z1, X1, X3, Y1, Z3, Y3), (Z3, X1, Y1, Y3, Z1, X3), (X1, Y3, Z3, Z1, X3, Y1), (X3, Z3, Z1, Y1, X1, Y3),
-    (Y1, X1, Z1, Z3, Y3, X3), (X3, Z3, X1, Y1, Y3, Z1), (Z3, X3, Z1, Y3, Y1, X1), (X1, Y3, X3, Z1, Z3, Y1),
-    (Z3, Z1, X1, Y3, X3, Y1), (Z1, X3, X1, Z3, Y3, Y1), (Y1, Z1, X3, X1, Y3, Z3), (Y3, Z1, X3, Z3, X1, Y1),
+    (Z3, X3, Y3, X1, Z1, Y1), (Z1, X3, X1, Y3, Z3, Y1), (X1, Y3, Z3, X3, Y1, Z1), (X3, X1, Z1, Z3, Y1, Y3),
+    (Y3, Z1, X3, Z3, X1, Y1), (Z1, X3, Z3, X1, Y3, Y1), (X3, Z3, Z1, X1, Y3, Y1), (Z3, Y1, X3, X1, Y3, Z1),
+    (X1, Z1, X3, Y3, Y1, Z3), (Y1, Z3, X1, Y3, X3, Z1), (Y1, Z1, Z3, X1, X3, Y3), (Z3, X1, Y1, Y3, X3, Z1),
 )
 AG_ORDERS = (
-    (X3, Z1, X1, Z3), (Z1, Z3, X3, X1), (X3, X1, Z3, Z1), (Z1, Z3, X3, X1), (Z3, X1, Z1, X3),
-    (Z3, X3, X1, Z1), (Z3, X3, Z1, X1), (Z1, Z3, X1, X3), (X1, X3, Z1, Z3), (X1, Z1, Z3, X3),
-    (Z1, X1, X3, Z3), (Z3, X3, X1, Z1),
+    (X1, Z1, Z3, X3), (X3, Z1, Z3, X1), (X1, X3, Z3, Z1), (X3, Z1, X1, Z3), (Z3, X1, X3, Z1),
+    (X3, Z3, Z1, X1), (X1, X3, Z1, Z3), (Z1, Z3, X3, X1), (Z1, X1, Z3, X3), (Z3, X1, Z1, X3),
+    (Z3, X1, Z1, X3), (Z1, X3, X1, Z3),
 )
-DIRECT = ((0, 0), (1, 3))
+DIRECT = ((0, 1), (1, 3))
 LEN = 768
 HALF = 384
 D = 2048
@@ -48,36 +48,35 @@
 START, ELEM, TURN, PROD, RS, AG, WY, WF, TAP, BACK, FIN = range(11)
 NAMES = ("start", "elem", "turn", "prod", "rs", "ag", "wy", "wf", "tap", "back", "fin")
 SCHEDULE = (
-    (ELEM, 0, 0, 1), (TURN, 0), (START,), (WY, 0, 0, Y1, 2, 0), (WY, 1, 0, Y3, 1, 0), (ELEM, 0, 1, 4),
-    (WY, 0, 0, Y1, 0, 0), (WY, 0, 0, Y3, 2, 0), (TURN, 1), (PROD, 0, 0), (WY, 0, 0, Y1, 3, 0),
-    (WY, 1, 0, Y3, 3, 0), (WF, 1, 3, 1), (PROD, 0, 1), (ELEM, 1, 0, 2), (WY, 1, 0, Y1, 0, 0),
-    (WY, 1, 0, Y3, 0, 0), (ELEM, 1, 2, 4), (PROD, 1, 0), (WY, 0, 0, Y3, 1, 0), (PROD, 1, 1), (ELEM, 2, 0, 1),
-    (WF, 0, 1, 2), (ELEM, 2, 1, 3), (WY, 0, 0, Y3, 0, 0), (PROD, 2, 0), (TAP, -1), (PROD, 2, 1), (RS, 0, 0),
-    (RS, 2, 0), (RS, 1, 0), (BACK, 0, 0), (RS, 3, 0), (BACK, 0, 1), (FIN, 0, 0), (FIN, 0, 1), (RS, 4, 0),
-    (WF, 0, 3, 2), (RS, 6, 0), (RS, 9, 0), (TAP, 0), (RS, 7, 0), (RS, 11, 0), (WY, 1, 0, Y1, 1, 0),
-    (RS, 5, 0), (RS, 10, 0), (WY, 0, 0, Y1, 1, 0), (RS, 0, 1), (RS, 2, 1), (RS, 8, 0), (RS, 11, 1),
-    (RS, 6, 1), (WY, 1, 0, Y1, 2, 0), (WY, 1, 0, Y3, 2, 0), (TAP, 1), (RS, 1, 1), (RS, 10, 1), (RS, 9, 1),
-    (RS, 3, 1), (RS, 7, 1), (WY, 0, 1, Y3, 1, 0), (RS, 0, 2), (RS, 8, 1), (RS, 11, 2), (RS, 4, 1),
-    (WY, 1, 0, Y1, 3, 0), (WY, 0, 1, Y3, 2, 0), (RS, 5, 1), (WF, 0, 1, 3), (WF, 0, 1, 1), (RS, 6, 2),
-    (RS, 10, 2), (RS, 1, 2), (RS, 9, 2), (RS, 0, 3), (RS, 2, 2), (TAP, 2), (WY, 1, 3, Y1, 0, 0), (RS, 3, 2),
-    (RS, 11, 3), (RS, 7, 2), (RS, 8, 2), (WF, 0, 3, 1), (WF, 1, 3, 0), (WF, 1, 3, 2), (RS, 4, 2), (RS, 5, 2),
-    (WY, 0, 0, Y3, 3, 0), (RS, 2, 3), (RS, 6, 3), (RS, 10, 3), (RS, 11, 4), (RS, 9, 3), (RS, 7, 3),
-    (WF, 1, 1, 0), (RS, 0, 4), (RS, 1, 3), (WF, 0, 2, 1), (RS, 8, 3), (WF, 1, 1, 2), (RS, 4, 3),
-    (WY, 1, 3, Y1, 1, 0), (TAP, 3), (RS, 3, 3), (RS, 7, 4), (RS, 5, 3), (RS, 2, 4), (RS, 1, 4), (RS, 6, 4),
-    (WY, 0, 1, Y3, 0, 0), (RS, 11, 5), (WF, 1, 2, 0), (WF, 0, 3, 3), (WF, 1, 1, 1), (RS, 10, 4),
-    (WF, 0, 2, 2), (RS, 9, 4), (RS, 0, 5), (WY, 1, 3, Y1, 2, 0), (RS, 4, 4), (AG, 11, 0), (RS, 3, 4),
-    (RS, 5, 4), (RS, 6, 5), (RS, 8, 4), (RS, 1, 5), (WY, 0, 1, Y3, 3, 0), (RS, 7, 5), (RS, 2, 5), (RS, 9, 5),
-    (WY, 1, 3, Y1, 3, 0), (WF, 1, 2, 1), (RS, 10, 5), (AG, 6, 0), (RS, 3, 5), (TAP, 4), (AG, 9, 0),
-    (WY, 1, 0, Y3, 3, 1), (AG, 0, 0), (RS, 4, 5), (RS, 5, 5), (WF, 1, 2, 2), (AG, 11, 1), (RS, 8, 5),
-    (AG, 1, 0), (AG, 2, 0), (AG, 7, 0), (AG, 10, 0), (WY, 0, 0, Y1, 0, 1), (AG, 3, 0), (AG, 9, 1), (AG, 4, 0),
-    (AG, 0, 1), (WF, 0, 2, 3), (AG, 5, 0), (WY, 0, 0, Y3, 0, 1), (AG, 1, 1), (AG, 11, 2), (AG, 8, 0),
-    (AG, 7, 1), (AG, 2, 1), (AG, 3, 1), (WY, 1, 0, Y1, 3, 1), (TAP, 5), (AG, 10, 1), (AG, 6, 1), (AG, 4, 1),
-    (AG, 5, 1), (AG, 9, 2), (BACK, 3, 1), (AG, 0, 2), (AG, 1, 2), (AG, 8, 1), (WY, 0, 1, Y3, 0, 1),
-    (BACK, 1, 0), (WY, 1, 3, Y1, 3, 1), (AG, 7, 2), (AG, 3, 2), (FIN, 3, 1), (AG, 11, 3), (AG, 6, 2),
-    (AG, 5, 2), (BACK, 3, 0), (AG, 2, 2), (AG, 4, 2), (AG, 10, 2), (FIN, 1, 0), (BACK, 1, 1), (AG, 8, 2),
-    (AG, 9, 3), (AG, 1, 3), (FIN, 3, 0), (AG, 0, 3), (BACK, 2, 0), (AG, 7, 3), (AG, 5, 3), (FIN, 1, 1),
-    (AG, 3, 3), (BACK, 2, 1), (AG, 10, 3), (FIN, 2, 0), (AG, 4, 3), (AG, 2, 3), (AG, 8, 3), (AG, 6, 3),
-    (FIN, 2, 1),
+    (ELEM, 0, 0, 2), (START,), (WY, 0, 0, Y1, 1, 0), (WY, 1, 0, Y3, 1, 0), (ELEM, 0, 2, 4), (TURN, 0),
+    (WY, 0, 0, Y1, 2, 0), (WY, 0, 0, Y3, 0, 0), (TURN, 1), (PROD, 0, 0), (WY, 0, 0, Y1, 3, 0),
+    (WY, 1, 0, Y3, 0, 0), (PROD, 0, 1), (ELEM, 1, 0, 2), (WY, 1, 0, Y1, 0, 0), (WY, 0, 1, Y3, 1, 0),
+    (ELEM, 1, 2, 4), (PROD, 1, 0), (WY, 1, 3, Y1, 1, 0), (PROD, 1, 1), (ELEM, 2, 0, 1), (ELEM, 2, 1, 3),
+    (WY, 1, 3, Y1, 0, 0), (WF, 1, 3, 0), (PROD, 2, 0), (TAP, -1), (PROD, 2, 1), (BACK, 0, 0), (BACK, 0, 1),
+    (RS, 1, 0), (RS, 0, 0), (WY, 0, 0, Y3, 1, 0), (FIN, 0, 0), (RS, 2, 0), (RS, 3, 0), (FIN, 0, 1),
+    (WF, 0, 1, 2), (RS, 4, 0), (RS, 5, 0), (RS, 7, 0), (RS, 6, 0), (RS, 9, 0), (RS, 8, 0),
+    (WY, 0, 0, Y3, 2, 0), (TAP, 0), (WF, 1, 2, 0), (RS, 2, 1), (RS, 1, 1), (WY, 0, 1, Y3, 2, 0), (RS, 11, 0),
+    (RS, 3, 1), (RS, 4, 1), (RS, 10, 0), (WY, 0, 1, Y3, 3, 0), (TAP, 1), (RS, 0, 1), (RS, 8, 1), (RS, 6, 1),
+    (WY, 1, 0, Y1, 2, 0), (RS, 1, 2), (RS, 3, 2), (WF, 1, 1, 0), (RS, 7, 1), (WY, 1, 0, Y1, 1, 0), (RS, 9, 1),
+    (RS, 5, 1), (RS, 11, 1), (WY, 0, 0, Y3, 3, 0), (WF, 0, 2, 2), (RS, 10, 1), (RS, 2, 2), (TAP, 2),
+    (RS, 4, 2), (RS, 0, 2), (RS, 3, 3), (RS, 1, 3), (RS, 6, 2), (RS, 8, 2), (WF, 0, 3, 2),
+    (WY, 0, 0, Y1, 0, 0), (WY, 1, 0, Y3, 2, 0), (RS, 5, 2), (WF, 1, 3, 1), (WF, 0, 1, 3), (RS, 9, 2),
+    (RS, 7, 2), (RS, 11, 2), (RS, 10, 2), (RS, 0, 3), (RS, 2, 3), (RS, 3, 4), (RS, 8, 3), (RS, 4, 3),
+    (WF, 1, 1, 2), (RS, 6, 3), (RS, 1, 4), (WF, 1, 1, 1), (TAP, 3), (WF, 0, 3, 3), (WY, 1, 0, Y1, 3, 1),
+    (RS, 5, 3), (WF, 0, 3, 0), (RS, 0, 4), (RS, 7, 3), (RS, 2, 4), (RS, 8, 4), (RS, 10, 3), (RS, 9, 3),
+    (RS, 1, 5), (WY, 1, 0, Y3, 3, 0), (RS, 4, 4), (WF, 1, 3, 2), (WF, 0, 2, 3), (RS, 11, 3), (WF, 0, 1, 0),
+    (RS, 3, 5), (WY, 1, 3, Y1, 2, 0), (RS, 6, 4), (WF, 1, 2, 1), (RS, 5, 4), (RS, 7, 4), (RS, 2, 5),
+    (RS, 10, 4), (RS, 8, 5), (RS, 0, 5), (RS, 9, 4), (WY, 0, 1, Y3, 0, 0), (TAP, 4), (RS, 4, 5), (AG, 1, 0),
+    (RS, 11, 4), (AG, 3, 0), (WY, 0, 0, Y1, 1, 1), (RS, 10, 5), (RS, 7, 5), (AG, 8, 0), (WY, 1, 0, Y3, 3, 1),
+    (RS, 9, 5), (AG, 2, 0), (RS, 6, 5), (AG, 0, 0), (AG, 1, 1), (RS, 5, 5), (AG, 4, 0), (RS, 11, 5), (TAP, 5),
+    (WY, 1, 3, Y1, 3, 0), (AG, 10, 0), (AG, 3, 1), (WF, 1, 2, 2), (AG, 7, 0), (AG, 8, 1), (AG, 9, 0),
+    (AG, 6, 0), (AG, 2, 1), (AG, 5, 0), (AG, 0, 1), (WY, 0, 0, Y3, 1, 1), (AG, 11, 0), (AG, 4, 1), (AG, 1, 2),
+    (AG, 10, 1), (BACK, 1, 0), (WY, 1, 0, Y1, 3, 0), (AG, 6, 1), (AG, 7, 1), (AG, 8, 2), (AG, 3, 2),
+    (WF, 0, 2, 0), (AG, 9, 1), (AG, 11, 1), (BACK, 3, 1), (WY, 0, 1, Y3, 1, 1), (FIN, 1, 0), (AG, 5, 1),
+    (AG, 4, 2), (AG, 2, 2), (AG, 10, 2), (WY, 1, 3, Y1, 3, 1), (AG, 1, 3), (FIN, 3, 1), (AG, 0, 2),
+    (AG, 7, 2), (AG, 6, 2), (BACK, 3, 0), (AG, 9, 2), (AG, 8, 3), (BACK, 1, 1), (FIN, 3, 0), (AG, 5, 2),
+    (AG, 3, 3), (AG, 10, 3), (AG, 11, 2), (BACK, 2, 0), (FIN, 1, 1), (AG, 6, 3), (AG, 4, 3), (BACK, 2, 1),
+    (FIN, 2, 0), (AG, 0, 3), (AG, 7, 3), (AG, 2, 3), (AG, 11, 3), (AG, 9, 3), (FIN, 2, 1), (AG, 5, 3),
 )
 
 

time: 114 us -> 113 us (level)
  no operation moved by 1% of the time
where the time goes in v4:
time: 113 us
  Pallas kernels  112 us (99%)
    pallas_call x1, Pallas kernels, fused(): pl.pallas_call(kernel, in_specs=[any_space] * 6 + [in_vmem] * 2, out_spec...  106 us
    pallas_call x1, Pallas kernels, finished(): pl.pallas_call(functools.partial(finish_kernel, factor), in_specs=[any_sp...  6.16 us

profile of v4, /device:TPU:1, one launch (start us, length us, event | category | flops | bytes accessed | tf_op | source)
XLA Modules:
  0.0 113.1 jit_solution(11577424398361536398)
XLA Ops:
  0.6 106.2 %shard_map.119 = (bf16[384,2048]{1,0:T(8,128)(2,1)}, f32[2,8,1408]{2,1,0:T(8,128)}, bf16[16,16,512]{2,1,0:T(8,128)(2,1)}, bf16[16,16,512]{2,1,0:T(8,128)(2,1)}, ...) custom-call(bf16[384,2048]{1,0:T(8,128)(2,1)} %bitcast.10, ...), custom_call_target="tpu_custom_call" | custom-call | flops 17999998976 | bytes 20971520 | tf_op jit(solution)/shard_map/pallas_call | solution.py:440
  106.8 6.2 %shard_map.120 = (bf16[384,2048]{1,0:T(8,128)(2,1)}, f32[512,1408]{1,0:T(8,128)}, f32[512,1408]{1,0:T(8,128)}, f32[3,2816]{1,0:T(4,128)}, f32[3,2816]{1,0:T(4,128)}) custom-call(bf16[384,2048]{1,0:T(8,128)(2,1)} %get-tuple-element.24.gin_hbm, f32[2,8,1408]{2,1,0:T(8,128)} %get-tuple-element.25.taps_ref, bf16[16,16,512]{2,1,0:T(8,128)(2,1)} %get-tuple-element.26.rest_0_, ...), custom_call_target="tpu_custom_call" | custom-call | tf_op jit(solution)/shard_map/pallas_call | solution.py:515
